TPU v7x, 256 devices: a whole 4x4x8 slice. The times are simulated.
256 devices in a mesh: row: 32 (over z, x), col: 8 (over y, core).
Axes of the slice: x: 4, y: 4, z: 8, core: 2. Of those that a mesh axis runs over, the one named last changes fastest.
Arguments:
- tokens: bfloat16 [8192, 2048], P('row'), may hold values from -6 to 6
- norm_gain: float32 [2048], replicated, may hold values from 0.5 to 1.5
- first_gate: bfloat16 [2048, 1024], P(None, 'col'), may hold values from -0.125 to 0.125
- second_gate: bfloat16 [2048, 1024], P(None, 'col'), may hold values from -0.125 to 0.125
- value_weight: bfloat16 [2048, 1024], P(None, 'col'), may hold values from -0.125 to 0.125
- short_weight: bfloat16 [3, 3, 1024], P(None, None, 'col'), may hold values from -3.5 to 3.5
- short_bias: float32 [3, 1024], P(None, 'col'), may hold values from -2 to 2
- embed_weight: float32 [33, 64], replicated, may hold values from -1 to 1
- embed_bias: float32 [64], replicated, may hold values from -3 to 3
- inner_weight: float32 [64, 64], replicated, may hold values from -0.75 to 0.75
- inner_bias: float32 [64], replicated, may hold values from -3 to 3
- filter_freq: float32 [64], replicated, may hold values from 0.5 to 1.5
- filter_weight: float32 [2, 2, 64, 1024], P(None, None, None, ('col', 'row')), may hold values from -0.0234375 to 0.0234375
- filter_skip: float32 [2, 1024], P(None, ('col', 'row')), may hold values from -3 to 3
- output_gain: float32 [1024], P('col'), may hold values from 0.5 to 1.5
- output_weight: bfloat16 [1024, 2048], replicated, may hold values from -0.1875 to 0.1875
Outputs:
- mixed_output: bfloat16 [8192, 2048], P(('row', 'col'))
All inputs are finite; a program needn't handle non-finite values.
Results may differ from a plain program's by a relative error of at most 0.01.
Values may be sent and summed in bfloat16 or wider, within the bound.
A program may use at most 64 MiB of HBM per device.

v0:
```python
import math

import jax
import jax.numpy as jnp
from jax import lax
from jax.sharding import PartitionSpec as P

CHANNELS = 1024
GROUPS = 8
FREQ_BANDS = 16


HIGHEST = lax.Precision.HIGHEST
NORM_EPS = 1e-06
DECAY_TARGET = 0.01
FAST_SPAN = 0.3
SLOW_SPAN = 1.5


def for_sending(value):
    return jax.tree.map(lambda a: a.astype(jnp.bfloat16) if a.dtype == jnp.float32 else a, value)


def position_features(length):
    position_ramp = jnp.linspace(0.0, 1.0, length, dtype=jnp.float32)[:, None]
    angles = 2.0 * math.pi * jnp.arange(length, dtype=jnp.float32)[:, None] / length
    band_freqs = jnp.linspace(0.0001, FREQ_BANDS - 1, FREQ_BANDS, dtype=jnp.float32)[None, :]
    features = jnp.concatenate(
        [position_ramp, jnp.cos(band_freqs * angles), -jnp.sin(band_freqs * angles)], axis=1
    )
    return (position_ramp, features)


def filter_hidden(length, embed_weight, embed_bias, inner_weight, inner_bias, filter_freq):
    position_ramp, features = position_features(length)
    hidden = jnp.sin(
        filter_freq * (jnp.dot(features, embed_weight, precision=HIGHEST) + embed_bias)
    )
    hidden = jnp.sin(filter_freq * (jnp.dot(hidden, inner_weight, precision=HIGHEST) + inner_bias))
    return (position_ramp, hidden)


def decay_rates():
    fastest = math.log(DECAY_TARGET) / FAST_SPAN
    slowest = math.log(DECAY_TARGET) / SLOW_SPAN
    return jnp.abs(jnp.linspace(slowest, fastest, CHANNELS, dtype=jnp.float32))


def short_filter(padded, weights, bias_row, length):
    result = bias_row.astype(jnp.float32)
    for tap_index in range(weights.shape[0]):
        result = result + padded[tap_index : tap_index + length].astype(jnp.float32) * weights[
            tap_index
        ].astype(jnp.float32)
    return result


def phase_table(rows, cols, period):
    phase_index = (
        lax.broadcasted_iota(jnp.int32, (rows, cols), 0)
        * lax.broadcasted_iota(jnp.int32, (rows, cols), 1)
        % period
    )
    phase_angle = phase_index.astype(jnp.float32) * (2.0 * math.pi / period)
    return (jnp.cos(phase_angle), jnp.sin(phase_angle))


def split_length(total_size):
    chosen = 2
    for candidate in range(2, math.isqrt(total_size) + 1, 2):
        if total_size % candidate == 0:
            chosen = candidate
    return chosen


def make_tables(total_size):
    major_size = split_length(total_size)
    minor_size = total_size // major_size
    inner_table = phase_table(major_size, major_size, major_size)
    twiddle = phase_table(major_size, minor_size, total_size)
    outer_table = phase_table(minor_size, minor_size, minor_size)
    return (major_size, minor_size, inner_table, twiddle, outer_table)


def finish_forward(part_real, part_imag, twiddle, outer_table):
    turn_cos = twiddle[0][:, :, None]
    turn_sin = twiddle[1][:, :, None]
    turned_real = part_real * turn_cos + part_imag * turn_sin
    turned_imag = part_imag * turn_cos - part_real * turn_sin
    outer_cos, outer_sin = outer_table
    spec_real = jnp.einsum("anc,nk->akc", turned_real, outer_cos, precision=HIGHEST) + jnp.einsum(
        "anc,nk->akc", turned_imag, outer_sin, precision=HIGHEST
    )
    spec_imag = jnp.einsum("anc,nk->akc", turned_imag, outer_cos, precision=HIGHEST) - jnp.einsum(
        "anc,nk->akc", turned_real, outer_sin, precision=HIGHEST
    )
    return (spec_real, spec_imag)


def forward_signal(signal, tables):
    major_size, minor_size, inner_table, twiddle, outer_table = tables
    channels = signal.shape[1]
    flattened = signal.reshape(major_size // 2, minor_size * channels)
    inner_cos = inner_table[0][:, : major_size // 2]
    inner_sin = inner_table[1][:, : major_size // 2]
    part_real = jnp.dot(inner_cos, flattened, precision=HIGHEST).reshape(
        major_size, minor_size, channels
    )
    part_imag = -jnp.dot(inner_sin, flattened, precision=HIGHEST).reshape(
        major_size, minor_size, channels
    )
    return finish_forward(part_real, part_imag, twiddle, outer_table)


def forward_taps(circular_taps, tables):
    major_size, minor_size, inner_table, twiddle, outer_table = tables
    channels = circular_taps.shape[1]
    flattened = circular_taps.reshape(major_size, minor_size * channels)
    part_real = jnp.dot(inner_table[0], flattened, precision=HIGHEST).reshape(
        major_size, minor_size, channels
    )
    part_imag = -jnp.dot(inner_table[1], flattened, precision=HIGHEST).reshape(
        major_size, minor_size, channels
    )
    return finish_forward(part_real, part_imag, twiddle, outer_table)


def inverse(spec_real, spec_imag, tables):
    major_size, minor_size, inner_table, twiddle, outer_table = tables
    channels = spec_real.shape[2]
    outer_cos, outer_sin = outer_table
    back_real = jnp.einsum("akc,kn->anc", spec_real, outer_cos, precision=HIGHEST) - jnp.einsum(
        "akc,kn->anc", spec_imag, outer_sin, precision=HIGHEST
    )
    back_imag = jnp.einsum("akc,kn->anc", spec_imag, outer_cos, precision=HIGHEST) + jnp.einsum(
        "akc,kn->anc", spec_real, outer_sin, precision=HIGHEST
    )
    turn_cos = twiddle[0][:, :, None]
    turn_sin = twiddle[1][:, :, None]
    turned_real = (back_real * turn_cos - back_imag * turn_sin).reshape(
        major_size, minor_size * channels
    )
    turned_imag = (back_imag * turn_cos + back_real * turn_sin).reshape(
        major_size, minor_size * channels
    )
    half_rows = major_size // 2
    values = jnp.dot(inner_table[0][:half_rows], turned_real, precision=HIGHEST) - jnp.dot(
        inner_table[1][:half_rows], turned_imag, precision=HIGHEST
    )
    return values.reshape(half_rows * minor_size, channels) / (major_size * minor_size)


def two_sided(signal, forward, backward, skip_gain, tables):
    circular_taps = jnp.concatenate([forward, jnp.zeros_like(forward[:1]), backward[:0:-1]], axis=0)
    signal_real, signal_imag = forward_signal(signal, tables)
    taps_real, taps_imag = forward_taps(circular_taps, tables)
    prod_real = signal_real * taps_real - signal_imag * taps_imag
    prod_imag = signal_real * taps_imag + signal_imag * taps_real
    return inverse(prod_real, prod_imag, tables) + signal * skip_gain


def channel_taps(hidden, position_ramp, filter_weight, deltas):
    window = jnp.exp(-position_ramp * deltas[None, :])
    pairs = []
    for order_index in range(filter_weight.shape[0]):
        forward = jnp.dot(hidden, filter_weight[order_index, 0], precision=HIGHEST) * window
        backward = jnp.dot(hidden, filter_weight[order_index, 1], precision=HIGHEST) * window
        pairs.append((forward, backward))
    return pairs


def local(
    tokens,
    norm_gain,
    first_gate,
    second_gate,
    value_weight,
    short_weight,
    short_bias,
    embed_weight,
    embed_bias,
    inner_weight,
    inner_bias,
    filter_freq,
    filter_weight,
    filter_skip,
    output_gain,
    output_weight,
):
    row_count = lax.axis_size("row")
    row_index = lax.axis_index("row")
    col_index = lax.axis_index("col")
    local_tokens = tokens.shape[0]
    length = local_tokens * row_count
    col_width = first_gate.shape[1]
    own_width = col_width // row_count
    widened = tokens.astype(jnp.float32)
    normed = (
        widened
        * lax.rsqrt(jnp.mean(widened * widened, axis=1, keepdims=True) + NORM_EPS)
        * norm_gain
    ).astype(jnp.bfloat16)
    gate_first = jnp.dot(normed, first_gate, preferred_element_type=jnp.float32).astype(
        jnp.bfloat16
    )
    gate_second = jnp.dot(normed, second_gate, preferred_element_type=jnp.float32).astype(
        jnp.bfloat16
    )
    gate_value = jnp.dot(normed, value_weight, preferred_element_type=jnp.float32).astype(
        jnp.bfloat16
    )
    position_ramp, hidden = filter_hidden(
        length, embed_weight, embed_bias, inner_weight, inner_bias, filter_freq
    )
    channel_start = (col_index * row_count + row_index) * own_width
    deltas = lax.dynamic_slice_in_dim(decay_rates(), channel_start, own_width)
    tap_pairs = channel_taps(hidden, position_ramp, filter_weight, deltas)
    tables = make_tables(2 * length)
    half_width = short_weight.shape[1] // 2
    moved = (
        lax.all_to_all(gate_first, "row", split_axis=1, concat_axis=0, tiled=True),
        lax.all_to_all(gate_second, "row", split_axis=1, concat_axis=0, tiled=True),
        lax.all_to_all(gate_value, "row", split_axis=1, concat_axis=0, tiled=True),
    )
    weights_own = lax.dynamic_slice_in_dim(short_weight, row_index * own_width, own_width, 2)
    bias_own = lax.dynamic_slice_in_dim(short_bias, row_index * own_width, own_width, 1)
    smoothed = [
        short_filter(
            jnp.pad(moved[branch], ((half_width, half_width), (0, 0))),
            weights_own[branch],
            bias_own[branch],
            length,
        )
        for branch in range(3)
    ]
    signal = smoothed[2]
    for order_index in range(2):
        signal = smoothed[order_index] * two_sided(
            signal,
            tap_pairs[order_index][0],
            tap_pairs[order_index][1],
            filter_skip[order_index],
            tables,
        )
    result = jax.tree.map(
        lambda part, own: part.astype(own.dtype),
        lax.all_to_all(for_sending(signal), "row", split_axis=0, concat_axis=1, tiled=True),
        signal,
    )
    group_width = CHANNELS // GROUPS
    grouped = result.reshape(local_tokens, col_width // group_width, group_width)
    scaled = grouped * lax.rsqrt(jnp.mean(grouped * grouped, axis=2, keepdims=True) + NORM_EPS)
    mix_local = (scaled.reshape(local_tokens, col_width) * output_gain).astype(jnp.bfloat16)
    gathered = lax.all_to_all(mix_local, "col", split_axis=0, concat_axis=1, tiled=True)
    return jnp.dot(gathered, output_weight, preferred_element_type=jnp.float32).astype(jnp.bfloat16)


def solution(mesh):
    in_specs = (
        P("row", None),
        P(),
        P(None, "col"),
        P(None, "col"),
        P(None, "col"),
        P(None, None, "col"),
        P(None, "col"),
        P(),
        P(),
        P(),
        P(),
        P(),
        P(None, None, None, ("col", "row")),
        P(None, ("col", "row")),
        P("col"),
        P(),
    )
    out_specs = P(("row", "col"), None)
    return jax.shard_map(local, mesh=mesh, in_specs=in_specs, out_specs=out_specs, check_vma=False)
```

profile of v0, /device:TPU:1, one launch (start us, length us, event | category | flops | bytes accessed | tf_op | source)
XLA Modules:
  0.0 213.7 jit_solution(14069972327601891070)
XLA Ops:
  0.0 1.6 fusion.4
  1.6 1.8 convolution_convert_fusion.1
  3.4 0.7 all_to_all.72
  4.1 12.0 %all-to-all-start.2 = ((bf16[256,32,4]{0,2,1:T(4,128)(2,1)}), bf16[256,32,4]{0,2,1:T(4,128)(2,1)}, u32[]{:S(2)}, u32[]{:S(2)}) async-start(bf16[256,32,4]{0,2,1:T(4,128)(2,1)} %all_to_all.72), calls=%async_computation.2 | async-start | bytes 131072 | tf_op jit(solution)/shard_map/all_to_all | solution.py:223
  16.2 0.9 fusion.96
  18.0 1.9 multiply_cosine_fusion
  20.0 8.7 %fusion.3 = f32[8192,64]{0,1:T(8,128)S(1)} fusion(f32[33,64]{1,0:T(8,128)S(1)} %copy-done.8, f32[8192,16]{0,1:T(8,128)S(1)} %get-tuple-element.16, f32[8192,16]{0,1:T(8,128)S(1)} %get-tuple-element.15, f32[8192,1]{0,1:T(1,128)S(1)} %bitcast.258, f32[64]{0:T(128)S(1)} %copy-done.14, f32[64]{0:T(128)S(1)} %copy-done.11), kind=kOutput, calls=%fused_computation.5 | convolution fusion | flops 209207296 | bytes 3187456 | tf_op jit(solution)/shard_map/dot_general | solution.py:37
  28.7 8.9 %fusion.1 = f32[8192,64]{0,1:T(8,128)S(1)} fusion(f32[8192,64]{0,1:T(8,128)S(1)} %fusion.3, f32[64,64]{1,0:T(8,128)S(1)} %copy-done.7, f32[64]{0:T(128)S(1)} %copy-done.15, f32[64]{0:T(128)S(1)} %copy-done.11), kind=kOutput, calls=%fused_computation.2 | convolution fusion | flops 403701760 | bytes 4211200 | tf_op jit(solution)/shard_map/dot_general | solution.py:39
  37.7 1.2 fusion.130
  38.9 1.2 convolution_multiply_fusion
  40.1 12.5 %convolution_multiply_fusion.1 = f32[8192,4]{0,1:T(4,128)S(1)} fusion(f32[8192,64]{0,1:T(8,128)S(1)} %fusion.1, f32[4]{0:T(128)S(1)} %dynamic_slice.11, f32[8192]{0:T(1024)S(1)} %get-tuple-element.17, f32[2,2,64,4]{2,3,1,0:T(4,128)S(1)} %copy-done.9), kind=kOutput, calls=%fused_computation.7 | convolution fusion | flops 25231360 | bytes 2263552 | tf_op jit(solution)/shard_map/dot_general | solution.py:166
  52.6 1.2 fusion.133
  54.1 5.6 %reverse = f32[8192,4]{0,1:T(4,128)S(1)} reverse(f32[8192,4]{0,1:T(4,128)S(1)} %bitcast.254), dimensions={0} | reverse | bytes 262144
  60.1 5.1 %copy.95 = f32[16384,4]{1,0:T(8,128)} copy(f32[16384,4]{0,1:T(4,128)S(1)} %concatenate.29) | data formatting | bytes 524288 | tf_op jit(solution)/shard_map/concatenate | solution.py:154
  65.2 8.3 %reshape.264 = f32[128,512]{1,0:T(8,128)S(1)} reshape(f32[16384,4]{1,0:T(8,128)} %copy.95) | data formatting | bytes 524288 | tf_op jit(solution)/shard_map/reshape | solution.py:118
  73.6 0.7 convolution_negate_fusion.2
  75.2 0.7 fusion.72
  75.8 0.7 fusion.76
  76.5 5.6 %reverse.1 = f32[8192,4]{0,1:T(4,128)S(1)} reverse(f32[8192,4]{0,1:T(4,128)S(1)} %bitcast.253), dimensions={0} | reverse | bytes 262144
  82.5 5.1 %copy.116 = f32[16384,4]{1,0:T(8,128)} copy(f32[16384,4]{0,1:T(4,128)S(1)} %concatenate.30) | data formatting | bytes 524288 | tf_op jit(solution)/shard_map/concatenate | solution.py:154
  87.6 8.3 %reshape.268 = f32[128,512]{1,0:T(8,128)S(1)} reshape(f32[16384,4]{1,0:T(8,128)} %copy.116) | data formatting | bytes 524288 | tf_op jit(solution)/shard_map/reshape | solution.py:118
  96.1 0.7 convolution_negate_fusion
  96.8 0.6 fusion.32
  97.4 1.4 fusion.62
  98.8 1.4 fusion.66
  100.2 2.3 %convolution_convert_fusion.2 = bf16[256,128]{0,1:T(8,128)(2,1)} fusion(bf16[2048,128]{1,0:T(8,128)(2,1)} %param.18, bf16[256,2048]{1,0:T(8,128)(2,1)S(1)} %copy-done.1, f32[2048]{0:T(1024)S(1)} %copy-done.18, f32[256]{0:T(256)S(1)} %add_rsqrt_fusion.1), kind=kOutput, calls=%fused_computation.44 | convolution fusion | flops 136347648 | bytes 1647616 | tf_op jit(solution)/shard_map/dot_general | solution.py:203
  102.5 1.2 convolution_convert_fusion.3
  103.7 0.7 convolution_subtract_fusion.4
  104.5 0.7 convolution_add_fusion.6
  105.2 0.7 convolution_subtract_fusion.1
  105.8 0.7 convolution_add_fusion.3
  106.7 0.7 all_to_all.68
  107.4 0.7 all_to_all.64
  108.3 9.6 %all-to-all-start.1 = ((bf16[256,32,4]{0,2,1:T(4,128)(2,1)}), bf16[256,32,4]{0,2,1:T(4,128)(2,1)S(1)}, u32[]{:S(2)}, u32[]{:S(2)}) async-start(bf16[256,32,4]{0,2,1:T(4,128)(2,1)} %all_to_all.68), calls=%async_computation.1 | async-start | bytes 131072 | tf_op jit(solution)/shard_map/all_to_all | solution.py:221
  117.9 1.1 multiply_add_fusion.8
  119.0 2.6 %copy.89 = f32[8192,4]{1,0:T(8,128)} copy(f32[8192,4]{0,1:T(4,128)S(1)} %multiply_add_fusion.8) | data formatting | bytes 262144 | tf_op jit(solution)/shard_map/add | solution.py:52
  121.6 5.0 %reshape.263 = f32[64,512]{1,0:T(8,128)S(1)} reshape(f32[8192,4]{1,0:T(8,128)} %copy.89) | data formatting | bytes 262144 | tf_op jit(solution)/shard_map/reshape | solution.py:103
  127.7 0.7 fusion.74
  128.4 0.7 fusion.78
  129.1 0.7 convolution_add_fusion.7
  129.8 0.7 multiply_subtract_fusion.5
  130.5 0.7 fusion.29
  131.3 0.7 fusion.25
  132.0 0.7 fusion.14
  132.8 0.7 multiply_add_fusion.4
  134.7 5.7 %div.58 = f32[8192,4]{1,0:T(8,128)} reshape(f32[64,512]{1,0:T(8,128)S(1)} %fusion.17) | data formatting | bytes 262144 | tf_op jit(solution)/shard_map/div | solution.py:150
  140.3 2.8 %copy.111 = f32[8192,4]{0,1:T(4,128)S(1)} copy(f32[8192,4]{1,0:T(8,128)} %div.58) | data formatting | bytes 262144 | tf_op jit(solution)/shard_map/div | solution.py:150
  143.2 9.5 %all-to-all-start = ((bf16[256,32,4]{0,2,1:T(4,128)(2,1)}), bf16[256,32,4]{0,2,1:T(4,128)(2,1)S(1)}, u32[]{:S(2)}, u32[]{:S(2)}) async-start(bf16[256,32,4]{0,2,1:T(4,128)(2,1)} %all_to_all.64), calls=%async_computation | async-start | bytes 131072 | tf_op jit(solution)/shard_map/all_to_all | solution.py:222
  152.7 1.2 add_multiply_fusion
  154.0 2.6 %copy.112 = f32[8192,4]{1,0:T(8,128)} copy(f32[8192,4]{0,1:T(4,128)S(1)} %add_multiply_fusion) | data formatting | bytes 262144 | tf_op jit(solution)/shard_map/mul | solution.py:238
  156.6 4.9 %reshape.267 = f32[64,512]{1,0:T(8,128)S(1)} reshape(f32[8192,4]{1,0:T(8,128)} %copy.112) | data formatting | bytes 262144 | tf_op jit(solution)/shard_map/reshape | solution.py:103
  162.6 0.7 fusion.64
  163.3 0.7 fusion.68
  164.0 0.7 convolution_add_fusion.4
  164.7 0.7 multiply_subtract_fusion.1
  165.5 0.7 fusion.23
  166.2 0.7 fusion.19
  167.0 0.7 fusion.12
  167.7 0.8 multiply_add_fusion
  169.6 5.7 %div.60 = f32[8192,4]{1,0:T(8,128)} reshape(f32[64,512]{1,0:T(8,128)S(1)} %fusion.16) | data formatting | bytes 262144 | tf_op jit(solution)/shard_map/div | solution.py:150
  175.3 2.9 %copy.132 = f32[8192,4]{0,1:T(4,128)S(1)} copy(f32[8192,4]{1,0:T(8,128)} %div.60) | data formatting | bytes 262144 | tf_op jit(solution)/shard_map/div | solution.py:150
  178.3 17.8 %all_to_all.86 = bf16[32,256,4]{1,2,0:T(4,128)(2,1)S(1)} all-to-all(bf16[32,256,4]{1,2,0:T(4,128)(2,1)S(1)} %bitcast.257), channel_id=1, replica_groups=mesh['row'=32,'col'=8] {'row'}, dimensions={0} | all-to-all | bytes 131072 | tf_op jit(solution)/shard_map/all_to_all | solution.py:247
  196.9 12.9 %all_to_all.87 = bf16[8,32,128]{2,1,0:T(8,128)(2,1)S(1)} all-to-all(bf16[8,32,128]{2,1,0:T(8,128)(2,1)S(1)} %copy.134), channel_id=1, replica_groups=mesh['row'=32,'col'=8] {'col'}, dimensions={0} | all-to-all | bytes 131072 | tf_op jit(solution)/shard_map/all_to_all | solution.py:254
  209.8 3.7 %convolution_convert_fusion = bf16[32,2048]{1,0:T(8,128)(2,1)} fusion(bf16[1024,2048]{1,0:T(8,128)(2,1)} %param.31, bf16[8,32,128]{2,1,0:T(8,128)(2,1)S(1)} %all_to_all.87), kind=kOutput, calls=%fused_computation.10 | convolution fusion | flops 134283264 | bytes 4390912 | tf_op jit(solution)/shard_map/dot_general | solution.py:255
  (92 shorter events, 9.0 us)
Async XLA Ops:
  0.0 1.6 copy-start
  1.6 18.4 %copy-start.8 = (f32[33,64]{1,0:T(8,128)S(1)}, f32[33,64]{1,0:T(8,128)}, u32[]{:S(2)}) copy-start(f32[33,64]{1,0:T(8,128)} %param.23) | copy-start | bytes 25348
  1.6 18.4 %copy-start.11 = (f32[64]{0:T(128)S(1)}, f32[64]{0:T(128)}, u32[]{:S(2)}) copy-start(f32[64]{0:T(128)} %param.27) | copy-start | bytes 772
  1.6 18.4 %copy-start.14 = (f32[64]{0:T(128)S(1)}, f32[64]{0:T(128)}, u32[]{:S(2)}) copy-start(f32[64]{0:T(128)} %param.24) | copy-start | bytes 772
  4.1 104.2 %all-to-all-start.2 = ((bf16[256,32,4]{0,2,1:T(4,128)(2,1)}), bf16[256,32,4]{0,2,1:T(4,128)(2,1)}, u32[]{:S(2)}, u32[]{:S(2)}) async-start(bf16[256,32,4]{0,2,1:T(4,128)(2,1)} %all_to_all.72), calls=%async_computation.2 | async-start | bytes 131072 | tf_op jit(solution)/shard_map/all_to_all | solution.py:223
  18.0 10.7 %copy-start.7 = (f32[64,64]{1,0:T(8,128)S(1)}, f32[64,64]{1,0:T(8,128)}, u32[]{:S(2)}) copy-start(f32[64,64]{1,0:T(8,128)} %param.25) | copy-start | bytes 49156
  18.0 10.7 %copy-start.15 = (f32[64]{0:T(128)S(1)}, f32[64]{0:T(128)}, u32[]{:S(2)}) copy-start(f32[64]{0:T(128)} %param.26) | copy-start | bytes 772
  28.7 9.0 %copy-start.9 = (f32[2,2,64,4]{2,3,1,0:T(4,128)S(1)}, f32[2,2,64,4]{2,3,1,0:T(4,128)}, u32[]{:S(2)}) copy-start(f32[2,2,64,4]{2,3,1,0:T(4,128)} %param.28) | copy-start | bytes 12292
  96.0 4.2 %copy-start.1 = (bf16[256,2048]{1,0:T(8,128)(2,1)S(1)}, bf16[256,2048]{1,0:T(8,128)(2,1)}, u32[]{:S(2)}) copy-start(bf16[256,2048]{1,0:T(8,128)(2,1)} %param.16) | copy-start | bytes 3145732
  96.0 4.2 %copy-start.18 = (f32[2048]{0:T(1024)S(1)}, f32[2048]{0:T(1024)}, u32[]{:S(2)}) copy-start(f32[2048]{0:T(1024)} %param.17) | copy-start | bytes 24580
  100.2 2.3 %copy-start.17 = (bf16[2048,128]{1,0:T(8,128)(2,1)S(1)}, bf16[2048,128]{1,0:T(8,128)(2,1)}, u32[]{:S(2)}) copy-start(bf16[2048,128]{1,0:T(8,128)(2,1)} %param.19) | copy-start | bytes 1572868
  102.5 2.6 %copy-start.3 = (f32[128,128,4]{1,0,2:T(8,128)S(1)}, f32[128,128,4]{1,0,2:T(8,128)}, u32[]{:S(2)}) copy-start(f32[128,128,4]{1,0,2:T(8,128)} %fusion.62) | copy-start | bytes 786436
  103.7 2.1 copy-start.2
  103.7 2.8 %copy-start.12 = (f32[3,128]{1,0:T(4,128)S(1)}, f32[3,128]{1,0:T(4,128)}, u32[]{:S(2)}) copy-start(f32[3,128]{1,0:T(4,128)} %param.22) | copy-start | bytes 4612
  103.7 2.9 %copy-start.13 = (f32[2,4]{1,0:T(2,128)S(1)}, f32[2,4]{1,0:T(2,128)}, u32[]{:S(2)}) copy-start(f32[2,4]{1,0:T(2,128)} %param.29) | copy-start | bytes 100
  103.7 2.9 %copy-start.10 = (bf16[3,3,128]{2,1,0:T(4,128)(2,1)S(1)}, bf16[3,3,128]{2,1,0:T(4,128)(2,1)}, u32[]{:S(2)}) copy-start(bf16[3,3,128]{2,1,0:T(4,128)(2,1)} %param.21) | copy-start | bytes 6916
  104.4 2.3 %copy-start.6 = (bf16[256,128]{0,1:T(8,128)(2,1)S(1)}, bf16[256,128]{0,1:T(8,128)(2,1)}, u32[]{:S(2)}) copy-start(bf16[256,128]{0,1:T(8,128)(2,1)} %convolution_convert_fusion.2) | copy-start | bytes 196612
  104.4 2.9 %copy-start.5 = (bf16[256,128]{0,1:T(8,128)(2,1)S(1)}, bf16[256,128]{0,1:T(8,128)(2,1)}, u32[]{:S(2)}) copy-start(bf16[256,128]{0,1:T(8,128)(2,1)} %convolution_convert_fusion.3) | copy-start | bytes 196612
  108.3 34.9 %all-to-all-start.1 = ((bf16[256,32,4]{0,2,1:T(4,128)(2,1)}), bf16[256,32,4]{0,2,1:T(4,128)(2,1)S(1)}, u32[]{:S(2)}, u32[]{:S(2)}) async-start(bf16[256,32,4]{0,2,1:T(4,128)(2,1)} %all_to_all.68), calls=%async_computation.1 | async-start | bytes 131072 | tf_op jit(solution)/shard_map/all_to_all | solution.py:221
  121.6 5.7 %copy-start.4 = (f32[128,128]{0,1:T(8,128)S(1)}, f32[128,128]{0,1:T(8,128)}, u32[]{:S(2)}) copy-start(f32[128,128]{0,1:T(8,128)} %fusion.96) | copy-start | bytes 196612
  143.2 35.0 %all-to-all-start = ((bf16[256,32,4]{0,2,1:T(4,128)(2,1)}), bf16[256,32,4]{0,2,1:T(4,128)(2,1)S(1)}, u32[]{:S(2)}, u32[]{:S(2)}) async-start(bf16[256,32,4]{0,2,1:T(4,128)(2,1)} %all_to_all.64), calls=%async_computation | async-start | bytes 131072 | tf_op jit(solution)/shard_map/all_to_all | solution.py:222
  175.3 21.2 %copy-start.16 = (f32[128]{0:T(128)S(1)}, f32[128]{0:T(128)}, u32[]{:S(2)}) copy-start(f32[128]{0:T(128)} %param.30) | copy-start | bytes 1540
where the time goes:
time: 218 us; the launch traced here: 214 us
  local copies, waits for them, and re-layouts  75.2 us (34%)
  matrix products  67.1 us (31%)
  starting transfers between devices  31.1 us (14%)
  blocking collectives  30.7 us (14%)
  other arithmetic  8.72 us (4%)
    all_to_all x1, blocking collectives, local(): lax.all_to_all(for_sending(signal), 'row', split_axis=0, concat_axis=1, t...  17.8 us
    div x4, local copies, waits for them, and re-layouts, inverse(): values.reshape(half_rows * minor_size, channels) / (major_size * minor_size)  17 us
    reshape x2, local copies, waits for them, and re-layouts, forward_taps(): flattened = circular_taps.reshape(major_size, minor_size * channels)  16.7 us
    dot_general x2, matrix products, channel_taps(): jnp.dot(hidden, filter_weight[order_index, 0], precision=HIGHEST) * window  13.7 us
    all_to_all x1, blocking collectives, local(): lax.all_to_all(mix_local, 'col', split_axis=0, concat_axis=1, tiled=True)  12.9 us
    all_to_all x1, starting transfers between devices, local(): lax.all_to_all(gate_value, 'row', split_axis=1, concat_axis=0, tiled=True)  12 us
    unnamed x42, local copies, waits for them, and re-layouts  11.5 us
    concatenate x4, local copies, waits for them, and re-layouts, two_sided(): jnp.concatenate([forward, jnp.zeros_like(forward[:1]), backward[:0:-1]],...  10.7 us
  transfers between devices with their start and end apart: 3, of which 0 were waited for; matrix products, arithmetic and copies ran while one was open for 66% of the time, Pallas kernels for 0%

commit v1 on v0

v1 whole, which is shorter than its diff:
```python
import math

import jax
import jax.numpy as jnp
import ml_dtypes
import numpy as np
from jax import lax
from jax.experimental import pallas as pl
from jax.experimental.pallas import tpu as pltpu
from jax.sharding import PartitionSpec as P

CHANNELS = 1024
GROUPS = 8
FREQ_BANDS = 16
NORM_EPS = 1e-06
DECAY_TARGET = 0.01
FAST_SPAN = 0.3
SLOW_SPAN = 1.5

LENGTH = 8192
WIDTH = 2048
COLS = 128
LIVE = 64
HALF = 72
TOTAL = 16384
ROWS = 32
OWN = 4
FEATS = 48
CHUNK = 2048

BF = jnp.bfloat16
F32 = jnp.float32
MESH = pl.DeviceIdType.MESH


def split_np(matrix):
    high = matrix.astype(np.float32).astype(ml_dtypes.bfloat16)
    low = (matrix - high.astype(np.float64)).astype(np.float32).astype(ml_dtypes.bfloat16)
    return high, low


def make_constants():
    k1 = np.arange(HALF)
    a = np.arange(LIVE)
    b = np.arange(COLS)
    cos_in = np.cos(2 * np.pi * np.outer(k1, a) / COLS)
    sin_in = np.sin(2 * np.pi * np.outer(k1, a) / COLS)
    first = np.concatenate([cos_in, -sin_in], 0)
    turn = 2 * np.pi * np.outer(k1, b) / TOTAL
    twiddle = np.concatenate([np.cos(turn), np.sin(turn)], 1).astype(np.float32)
    cos_out = np.cos(2 * np.pi * (np.outer(b, b) % COLS) / COLS)
    sin_out = np.sin(2 * np.pi * (np.outer(b, b) % COLS) / COLS)
    second = np.block([[cos_out, -sin_out], [sin_out, cos_out]])
    back = np.block([[cos_out, sin_out], [-sin_out, cos_out]])
    weight = np.where((k1 == 0) | (k1 == COLS // 2), 1.0, 2.0) * (k1 <= COLS // 2)
    last = np.concatenate([cos_in.T * weight, -sin_in.T * weight], 1) / TOTAL
    first_h, first_l = split_np(first)
    last_h, last_l = split_np(last)
    n = np.arange(LENGTH)
    ramp = np.linspace(0.0, 1.0, LENGTH)[None, :]
    bands = np.linspace(0.0001, FREQ_BANDS - 1, FREQ_BANDS, dtype=np.float32).astype(np.float64)
    angle = bands[:, None] * (2 * np.pi * n / LENGTH)[None, :]
    feats = np.zeros((FEATS, LENGTH))
    feats[0:1] = ramp
    feats[1 : 1 + FREQ_BANDS] = np.cos(angle)
    feats[1 + FREQ_BANDS : 1 + 2 * FREQ_BANDS] = -np.sin(angle)
    feats[1 + 2 * FREQ_BANDS] = 1.0
    return dict(
        first=np.concatenate([first_h, first_l, first_h], 1),
        twiddle=twiddle,
        second=np.stack(split_np(second)),
        back=np.stack(split_np(back)),
        last=np.concatenate([last_h, last_l, last_h], 1),
        feats=np.concatenate(split_np(feats), 0),
    )


def sine_coefficients():
    v = 0.25 * np.cos(np.pi * (np.arange(400) + 0.5) / 800)
    basis = np.stack([v ** (2 * j + 1) for j in range(5)], 1)
    scale = 1.0 / np.sin(2 * np.pi * v)
    found = np.linalg.lstsq(basis * scale[:, None], np.ones_like(v), rcond=None)[0]
    return [float(c) for c in found]


SINE = sine_coefficients()


def sine_of_turns(turns):
    v = 0.25 - jnp.abs(turns - jnp.round(turns))
    square = v * v
    result = SINE[4]
    for c in SINE[3::-1]:
        result = result * square + c
    return result * v


def split(value):
    high = value.astype(BF)
    return high, (value - high.astype(F32)).astype(BF)


def dot(left, right):
    return jnp.dot(left, right, preferred_element_type=F32)


def tall(value):
    high, low = split(value)
    return jnp.concatenate([high, high, low], axis=0)


def wide(value):
    high, low = split(value)
    return jnp.concatenate([high, low, high], axis=1)


def dot_table(value, table, lo, hi):
    high, low = split(value)
    return (
        dot(high, table[0, :, lo:hi]) + dot(low, table[0, :, lo:hi]) + dot(high, table[1, :, lo:hi])
    )


def into_spectrum(signal, first, twiddle):
    part = dot(first[...], tall(signal))
    cos, sin = twiddle[:, :COLS], twiddle[:, COLS:]
    pieces = []
    for i in range(OWN):
        real = part[:HALF, i * COLS : (i + 1) * COLS]
        imag = part[HALF:, i * COLS : (i + 1) * COLS]
        pieces.append(jnp.concatenate([real * cos + imag * sin, imag * cos - real * sin], axis=1))
    return jnp.concatenate(pieces, axis=0)


def from_spectrum(spectrum, back, last, twiddle):
    part = dot_table(spectrum, back, 0, 2 * COLS)
    cos, sin = twiddle[:, :COLS], twiddle[:, COLS:]
    reals, imags = [], []
    for i in range(OWN):
        real = part[i * HALF : (i + 1) * HALF, :COLS]
        imag = part[i * HALF : (i + 1) * HALF, COLS:]
        reals.append(real * cos - imag * sin)
        imags.append(real * sin + imag * cos)
    turned = jnp.concatenate(
        [jnp.concatenate(reals, axis=1), jnp.concatenate(imags, axis=1)], axis=0
    )
    return dot(last[...], tall(turned))


def kernel(
    tokens_hbm, norm_gain_hbm, gate0_hbm, gate1_hbm, gate2_hbm, short_w_hbm, short_b_hbm,
    embed_w_hbm, embed_b_hbm, inner_w_hbm, inner_b_hbm, freq_hbm, filter_w_hbm, skip_hbm,
    out_gain_hbm, out_w_hbm, first_hbm, twiddle_hbm, second_hbm, back_hbm, last_hbm, feats_hbm,
    out_ref,
    tokens, norm_gain, gates, short_w, short_b, embed_w, embed_b, inner_w, inner_b, freq,
    filter_w, skip, out_gain, out_w, first, twiddle, second, back, last, feats,
    normed, flat, packed, send1, recv1, params, mixed_taps, spectra, smooth,
    send2, recv2, send3, recv3, load_sem, send_sems, recv_sems,
):
    me = lax.axis_index("row")
    col = lax.axis_index("col")
    n_col = 8

    barrier = pltpu.get_barrier_semaphore()

    def greet_row(k, carry):
        pl.semaphore_signal(
            barrier, inc=1, device_id=(lax.rem(me + k, ROWS), col), device_id_type=MESH
        )
        return carry

    def greet_col(k, carry):
        pl.semaphore_signal(
            barrier, inc=1, device_id=(me, lax.rem(col + k, n_col)), device_id_type=MESH
        )
        return carry

    lax.fori_loop(1, ROWS, greet_row, 0)
    lax.fori_loop(1, n_col, greet_col, 0)

    loads = [
        pltpu.make_async_copy(src, dst, load_sem.at[j])
        for j, (src, dst) in enumerate(
            [
                (tokens_hbm, tokens),
                (norm_gain_hbm, norm_gain),
                (gate0_hbm, gates.at[:, 0:128]),
                (gate1_hbm, gates.at[:, 128:256]),
                (gate2_hbm, gates.at[:, 256:384]),
                (embed_w_hbm, embed_w),
                (embed_b_hbm, embed_b),
                (inner_w_hbm, inner_w),
                (inner_b_hbm, inner_b),
                (freq_hbm, freq),
                (filter_w_hbm, filter_w),
                (feats_hbm, feats),
                (first_hbm, first),
                (twiddle_hbm, twiddle),
                (second_hbm, second),
                (short_w_hbm, short_w),
                (short_b_hbm, short_b),
                (skip_hbm, skip),
                (back_hbm, back),
                (last_hbm, last),
                (out_gain_hbm, out_gain),
                (out_w_hbm, out_w),
            ]
        )
    ]
    for load in loads:
        load.start()

    for load in loads[0:2]:
        load.wait()

    def normalise(j, carry):
        rows = pl.ds(pl.multiple_of(j * 64, 64), 64)
        wide_tokens = tokens[rows, :].astype(F32)
        mean = jnp.mean(wide_tokens * wide_tokens, axis=1, keepdims=True)
        normed[rows, :] = (wide_tokens * lax.rsqrt(mean + NORM_EPS) * norm_gain[...]).astype(BF)
        return carry

    lax.fori_loop(0, 4, normalise, 0)
    for load in loads[2:5]:
        load.wait()
    projected = dot(normed[...], gates[...])
    projected = projected.astype(BF).astype(F32).T
    for b in range(3):
        for half in range(2):
            flat[pl.ds(half * 128, 128), :] = projected[
                b * 128 : (b + 1) * 128, half * 128 : (half + 1) * 128
            ]
        for half in range(2):
            for i in range(OWN):
                packed[pl.ds(4 * half + i, ROWS, stride=8), :] = flat[
                    pl.ds(128 * half + i, ROWS, stride=4), :
                ]
        send1[:, b] = packed[...].reshape(ROWS, 8, COLS).astype(BF)

    pl.semaphore_wait(barrier, ROWS - 1 + n_col - 1)

    def row_copy(source, target, number, k):
        there = lax.rem(me + k, ROWS)
        return pltpu.make_async_remote_copy(
            src_ref=source.at[there],
            dst_ref=target.at[me],
            send_sem=send_sems.at[number],
            recv_sem=recv_sems.at[number],
            device_id=(there, col),
            device_id_type=MESH,
        )

    def send_out(k, carry):
        row_copy(send1, recv1, 0, k).start()
        return carry

    lax.fori_loop(1, ROWS, send_out, 0)
    recv1[me] = send1[me]

    for load in loads[5:15]:
        load.wait()
    params[...] = jnp.zeros_like(params)
    scale = freq[...] * (1.0 / (2.0 * math.pi))
    params[0:33, 0:64] = embed_w[...] * scale
    params[33:34, 0:64] = embed_b[...] * scale - 0.25
    params[48:49, 0:64] = inner_b[...] * scale - 0.25
    params[64:128, 0:64] = inner_w[...] * scale
    params[0:64, 64:80] = jnp.concatenate(
        [filter_w[o, e] for o in range(2) for e in range(2)], axis=1
    )
    turned = params[...].T
    embed_t = wide(turned[0:64, 0:FEATS])
    inner_bias = turned[0:64, 48:49]
    inner_t = wide(turned[0:64, 64:128])
    filter_t = wide(turned[64:80, 0:64])

    row8 = lax.broadcasted_iota(jnp.int32, (8, 1), 0)
    channel = (col * ROWS + me) * OWN + lax.rem(row8, OWN)
    fastest = math.log(DECAY_TARGET) / FAST_SPAN
    slowest = math.log(DECAY_TARGET) / SLOW_SPAN
    place = channel.astype(F32) * (1.0 / (CHANNELS - 1))
    decay = jnp.abs(slowest * (1.0 - place) + fastest * place)

    def taps_of(j, carry):
        start = pl.multiple_of(j * CHUNK, CHUNK)
        lanes = pl.ds(start, CHUNK)
        high, low = feats[0:FEATS, lanes], feats[FEATS:, lanes]
        hidden = sine_of_turns(dot(embed_t, jnp.concatenate([high, high, low], axis=0)))
        hidden = sine_of_turns(dot(inner_t, tall(hidden)) + inner_bias)
        taps = dot(filter_t, tall(hidden))
        lag = start + lax.broadcasted_iota(jnp.int32, (8, CHUNK), 1)
        row = lax.broadcasted_iota(jnp.int32, (8, CHUNK), 0)
        window = jnp.exp(-(lag.astype(F32) * (1.0 / (LENGTH - 1))) * decay)
        window = jnp.where((lag == 0) & (row >= OWN), 0.0, window)
        for o in range(2):
            both = taps[8 * o : 8 * o + 8] * window
            other = pltpu.roll(both, OWN, axis=0)
            both = jnp.where(row < OWN, both + other, other - both)
            for q in range(CHUNK // COLS):
                at = pl.multiple_of(start // COLS * 8, 8) + o * LIVE * 8 + q * 8
                mixed_taps[pl.ds(pl.multiple_of(at, 8), 8), :] = both[:, q * COLS : (q + 1) * COLS]
        return carry

    lax.fori_loop(0, LENGTH // CHUNK, taps_of, 0)
    for o in range(2):
        for part in range(2):
            signal = jnp.concatenate(
                [
                    mixed_taps[pl.ds(o * LIVE * 8 + part * OWN + i, LIVE, stride=8), :]
                    for i in range(OWN)
                ],
                axis=1,
            )
            spectra[o, :, part * COLS : (part + 1) * COLS] = dot_table(
                into_spectrum(signal, first, twiddle), second, part * COLS, (part + 1) * COLS
            )

    for load in loads[15:21]:
        load.wait()
    lane8 = lax.broadcasted_iota(jnp.int32, (8, COLS), 1)
    mine = lane8 == OWN * me + lax.rem(lax.broadcasted_iota(jnp.int32, (8, COLS), 0), OWN)

    def own_column(line):
        return jnp.sum(
            jnp.where(mine, jnp.broadcast_to(line, (8, COLS)), 0.0), axis=1, keepdims=True
        )

    all_short = short_w[...].astype(F32)
    columns = [
        [own_column(all_short[b, j : j + 1]) for j in range(3)] + [own_column(short_b[b : b + 1, :])]
        for b in range(3)
    ]

    def wait_row(target, number):
        pltpu.make_async_copy(
            target.at[pl.ds(0, ROWS - 1)], target.at[pl.ds(0, ROWS - 1)], recv_sems.at[number]
        ).wait()

    wait_row(recv1, 0)
    row = lax.broadcasted_iota(jnp.int32, (256, COLS), 0)
    lane = lax.broadcasted_iota(jnp.int32, (256, COLS), 1)
    smoothed = []
    for b in range(3):
        here = recv1[:, b].astype(F32).reshape(256, COLS)
        before = pltpu.roll(here, 1, axis=1)
        before = jnp.where(lane == 0, pltpu.roll(before, OWN, axis=0), before)
        before = jnp.where((lane == 0) & (row < OWN), 0.0, before)
        after = pltpu.roll(here, COLS - 1, axis=1)
        after = jnp.where(lane == COLS - 1, pltpu.roll(after, 256 - OWN, axis=0), after)
        after = jnp.where((lane == COLS - 1) & (row >= 256 - OWN), 0.0, after)
        tap = [jnp.broadcast_to(c, (8, COLS))[None] for c in columns[b]]
        shape = (ROWS, 8, COLS)
        value = tap[3] + before.reshape(shape) * tap[0]
        value = value + here.reshape(shape) * tap[1]
        value = value + after.reshape(shape) * tap[2]
        smooth[b] = value.reshape(256, COLS)
        smoothed.append(
            jnp.concatenate(
                [smooth[b, pl.ds(i, LIVE, stride=OWN), :] for i in range(OWN)], axis=1
            )
        )

    signal = smoothed[2]
    for o in range(2):
        spectrum = dot_table(into_spectrum(signal, first, twiddle), second, 0, 2 * COLS)
        real, imag = spectrum[:, :COLS], spectrum[:, COLS:]
        t_real, t_imag = spectra[o, :, :COLS], spectra[o, :, COLS:]
        product = jnp.concatenate(
            [real * t_real - imag * t_imag, real * t_imag + imag * t_real], axis=1
        )
        direct = jnp.concatenate(
            [
                signal[:, i * COLS : (i + 1) * COLS]
                * jnp.broadcast_to(skip[o : o + 1, i : i + 1], (LIVE, COLS))
                for i in range(OWN)
            ],
            axis=1,
        )
        signal = smoothed[o] * (from_spectrum(product, back, last, twiddle) + direct)

    for i in range(OWN):
        flat[pl.ds(i * LIVE, LIVE), :] = signal[:, i * COLS : (i + 1) * COLS]
    for i in range(OWN):
        for half in range(2):
            packed[pl.ds(2 * i + half, ROWS, stride=8), :] = flat[
                pl.ds(i * LIVE + half, ROWS, stride=2), :
            ]
    send2[...] = packed[...].reshape(ROWS, 8, COLS).astype(BF)

    def send_back(k, carry):
        row_copy(send2, recv2, 1, k).start()
        return carry

    lax.fori_loop(1, ROWS, send_back, 0)
    recv2[me] = send2[me]
    wait_row(recv2, 1)

    values = recv2[...].astype(F32)
    squares = jnp.sum(values * values, axis=0)
    squares = squares + pltpu.roll(squares, 4, axis=0)
    squares = squares + pltpu.roll(squares, 2, axis=0)
    factor = lax.rsqrt(squares * (GROUPS / CHANNELS) + NORM_EPS)
    flat[...] = (values * factor[None]).reshape(256, COLS)
    for half in range(2):
        turned = flat[pl.ds(half, COLS, stride=2), :].T * out_gain[...]
        send3[4 * half : 4 * half + 4] = turned.reshape(4, 32, COLS).astype(BF)

    def send_over(k, carry):
        there = lax.rem(col + k, n_col)
        pltpu.make_async_remote_copy(
            src_ref=send3.at[there],
            dst_ref=recv3.at[col],
            send_sem=send_sems.at[2],
            recv_sem=recv_sems.at[2],
            device_id=(me, there),
            device_id_type=MESH,
        ).start()
        return carry

    lax.fori_loop(1, n_col, send_over, 0)
    recv3[col] = send3[col]
    loads[21].wait()
    pltpu.make_async_copy(
        recv3.at[pl.ds(0, n_col - 1)], recv3.at[pl.ds(0, n_col - 1)], recv_sems.at[2]
    ).wait()
    mixed = jnp.concatenate([recv3[c] for c in range(n_col)], axis=1)
    for q in range(4):
        out_ref[:, q * 512 : (q + 1) * 512] = dot(mixed, out_w[:, q * 512 : (q + 1) * 512]).astype(
            BF
        )

    for number, source in ((0, send1), (1, send2)):
        pltpu.make_async_copy(
            source.at[pl.ds(0, ROWS - 1)], source.at[pl.ds(0, ROWS - 1)], send_sems.at[number]
        ).wait()
    pltpu.make_async_copy(
        send3.at[pl.ds(0, n_col - 1)], send3.at[pl.ds(0, n_col - 1)], send_sems.at[2]
    ).wait()


def local(
    tokens, norm_gain, first_gate, second_gate, value_weight, short_weight, short_bias,
    embed_weight, embed_bias, inner_weight, inner_bias, filter_freq, filter_weight, filter_skip,
    output_gain, output_weight,
):
    constants = make_constants()
    operands = [
        tokens, norm_gain[None], first_gate, second_gate, value_weight, short_weight, short_bias,
        embed_weight, embed_bias[None], inner_weight, inner_bias[None], filter_freq[None],
        filter_weight, filter_skip, output_gain[None], output_weight,
    ] + [
        jnp.asarray(constants[name])
        for name in ("first", "twiddle", "second", "back", "last", "feats")
    ]
    vmem = pltpu.VMEM
    scratch = (
        [vmem(x.shape, x.dtype) for x in operands[0:2]]
        + [vmem((WIDTH, 384), BF)]
        + [vmem(x.shape, x.dtype) for x in operands[5:]]
    )
    scratch += [
        vmem((256, WIDTH), BF),
        vmem((256, COLS), F32),
        vmem((256, COLS), F32),
        vmem((ROWS, 3, 8, COLS), BF),
        vmem((ROWS, 3, 8, COLS), BF),
        vmem((128, 128), F32),
        vmem((2 * LIVE * 8, COLS), F32),
        vmem((2, OWN * HALF, 2 * COLS), F32),
        vmem((3, 256, COLS), F32),
        vmem((ROWS, 8, COLS), BF),
        vmem((ROWS, 8, COLS), BF),
        vmem((8, 32, COLS), BF),
        vmem((8, 32, COLS), BF),
        pltpu.SemaphoreType.DMA((22,)),
        pltpu.SemaphoreType.DMA((3,)),
        pltpu.SemaphoreType.DMA((3,)),
    ]
    return pl.pallas_call(
        kernel,
        out_shape=jax.ShapeDtypeStruct((32, WIDTH), BF),
        in_specs=[pl.BlockSpec(memory_space=pl.ANY)] * len(operands),
        out_specs=pl.BlockSpec(memory_space=pltpu.VMEM),
        scratch_shapes=scratch,
        compiler_params=pltpu.CompilerParams(
            collective_id=0, has_side_effects=True, vmem_limit_bytes=48 * 1024 * 1024
        ),
    )(*operands)


def solution(mesh):
    in_specs = (
        P("row", None),
        P(),
        P(None, "col"),
        P(None, "col"),
        P(None, "col"),
        P(None, None, "col"),
        P(None, "col"),
        P(),
        P(),
        P(),
        P(),
        P(),
        P(None, None, None, ("col", "row")),
        P(None, ("col", "row")),
        P("col"),
        P(),
    )
    out_specs = P(("row", "col"), None)
    return jax.shard_map(local, mesh=mesh, in_specs=in_specs, out_specs=out_specs, check_vma=False)
```

time: 218 us -> 53.1 us (0.24); the launches traced: 214 us -> 52.3 us
  matrix products: 67.1 us -> 0 us
  local copies, waits for them, and re-layouts: 75.2 us -> 18.6 us
  Pallas kernels: 0 us -> 33.7 us
  starting transfers between devices: 31.1 us -> 0 us
  blocking collectives: 30.7 us -> 0 us
  other arithmetic: 8.72 us -> 0 us
    dot_general x46 -> x0, matrix products: 67.1 us -> none  [the longest x2 13.7 us: channel_taps(): jnp.dot(hidden, filter_weight[order_index, 0], precision=HIGHEST) * window]
    pallas_call x0 -> x1, Pallas kernels: none -> 33.7 us  [local(): pl.pallas_call(kernel, out_shape=jax.ShapeDtypeStruct((32, WIDTH), BF), i...]
    all_to_all x3 -> x0, starting transfers between devices: 31.1 us -> none  [the longest x1 12 us: local(): lax.all_to_all(gate_value, 'row', split_axis=1, concat_axis=0, tiled=True)]
    all_to_all x2 -> x0, blocking collectives: 30.7 us -> none  [the longest x1 17.8 us: local(): lax.all_to_all(for_sending(signal), 'row', split_axis=0, concat_axis=1, t...]
    reshape x4 -> x0, local copies, waits for them, and re-layouts: 26.6 us -> none  [the longest x2 16.7 us: forward_taps(): flattened = circular_taps.reshape(major_size, minor_size * channels)]
    div x4 -> x0, local copies, waits for them, and re-layouts: 17 us -> none  [inverse(): values.reshape(half_rows * minor_size, channels) / (major_size * minor_size)]
    concatenate x4 -> x0, local copies, waits for them, and re-layouts: 10.7 us -> none  [two_sided(): jnp.concatenate([forward, jnp.zeros_like(forward[:1]), backward[:0:-1]],...]
    unnamed x42, local copies, waits for them, and re-layouts: 11.5 us -> 18.6 us
  transfers between devices with their start and end apart: 3 -> 0, of which waited for: 0 -> 0; matrix products, arithmetic and copies ran while one was open for 66% -> 0% of each run, Pallas kernels for 0% -> 0%
where the time goes in v1:
time: 53.1 us; the launch traced here: 52.3 us
  Pallas kernels  33.7 us (63%)
  local copies, waits for them, and re-layouts  18.6 us (35%)
    pallas_call x1, Pallas kernels, local(): pl.pallas_call(kernel, out_shape=jax.ShapeDtypeStruct((32, WIDTH), BF), i...  33.7 us
    unnamed x42, local copies, waits for them, and re-layouts  18.6 us

profile of v1, /device:TPU:1, one launch (start us, length us, event | category | flops | bytes accessed | tf_op | source)
XLA Modules:
  0.0 52.3 jit_solution(7061049251560132713)
XLA Ops:
  0.0 0.8 %copy.23.filter_w_hbm = f32[2,2,64,4]{3,2,1,0:T(8,128)S(1)} copy(f32[2,2,64,4]{2,3,1,0:T(4,128)} %param.34) | data formatting | bytes 8192 | tf_op args[12]
  0.8 0.0 copy-start
  0.8 1.4 %copy-done = bf16[96,8192]{1,0:T(8,128)(2,1)S(1)} copy-done((bf16[96,8192]{1,0:T(8,128)(2,1)S(1)}, bf16[96,8192]{1,0:T(8,128)(2,1)}, u32[]{:S(2)}) %copy-start) | copy-done | bytes 1572888
  2.2 0.0 copy-start.1
  2.2 1.2 %copy-done.1 = bf16[256,2048]{1,0:T(8,128)(2,1)S(1)} copy-done((bf16[256,2048]{1,0:T(8,128)(2,1)S(1)}, bf16[256,2048]{1,0:T(8,128)(2,1)}, u32[]{:S(2)}) %copy-start.1) | copy-done | bytes 1048600
  3.4 0.0 copy-start.2
  3.5 1.0 %copy-done.2 = bf16[2048,128]{1,0:T(8,128)(2,1)S(1)} copy-done((bf16[2048,128]{1,0:T(8,128)(2,1)S(1)}, bf16[2048,128]{1,0:T(8,128)(2,1)}, u32[]{:S(2)}) %copy-start.2) | copy-done | bytes 524312
  4.5 0.0 copy-start.3
  4.5 1.0 %copy-done.3 = bf16[2048,128]{1,0:T(8,128)(2,1)S(1)} copy-done((bf16[2048,128]{1,0:T(8,128)(2,1)S(1)}, bf16[2048,128]{1,0:T(8,128)(2,1)}, u32[]{:S(2)}) %copy-start.3) | copy-done | bytes 524312
  5.5 0.0 copy-start.4
  5.5 1.0 %copy-done.4 = bf16[2048,128]{1,0:T(8,128)(2,1)S(1)} copy-done((bf16[2048,128]{1,0:T(8,128)(2,1)S(1)}, bf16[2048,128]{1,0:T(8,128)(2,1)}, u32[]{:S(2)}) %copy-start.4) | copy-done | bytes 524312
  6.6 0.0 copy-start.5
  6.6 0.9 %copy-done.5 = bf16[2,256,256]{2,1,0:T(8,128)(2,1)S(1)} copy-done((bf16[2,256,256]{2,1,0:T(8,128)(2,1)S(1)}, bf16[2,256,256]{2,1,0:T(8,128)(2,1)}, u32[]{:S(2)}) %copy-start.5) | copy-done | bytes 262168
  7.5 0.0 copy-start.6
  7.5 0.9 %copy-done.6 = bf16[2,256,256]{2,1,0:T(8,128)(2,1)S(1)} copy-done((bf16[2,256,256]{2,1,0:T(8,128)(2,1)S(1)}, bf16[2,256,256]{2,1,0:T(8,128)(2,1)}, u32[]{:S(2)}) %copy-start.6) | copy-done | bytes 262168
  8.5 0.0 copy-start.7
  8.5 0.9 %copy-done.7 = f32[72,256]{1,0:T(8,128)S(1)} copy-done((f32[72,256]{1,0:T(8,128)S(1)}, f32[72,256]{1,0:T(8,128)}, u32[]{:S(2)}) %copy-start.7) | copy-done | bytes 73752
  9.4 0.0 copy-start.8
  9.4 0.9 %copy-done.8 = bf16[144,192]{1,0:T(8,128)(2,1)S(1)} copy-done((bf16[144,192]{1,0:T(8,128)(2,1)S(1)}, bf16[144,192]{1,0:T(8,128)(2,1)}, u32[]{:S(2)}) %copy-start.8) | copy-done | bytes 55320
  10.2 0.0 copy-start.9
  10.2 0.8 %copy-done.9 = bf16[64,432]{1,0:T(8,128)(2,1)S(1)} copy-done((bf16[64,432]{1,0:T(8,128)(2,1)S(1)}, bf16[64,432]{1,0:T(8,128)(2,1)}, u32[]{:S(2)}) %copy-start.9) | copy-done | bytes 55320
  11.1 0.0 copy-start.10
  11.1 0.8 %copy-done.10 = f32[64,64]{1,0:T(8,128)S(1)} copy-done((f32[64,64]{1,0:T(8,128)S(1)}, f32[64,64]{1,0:T(8,128)}, u32[]{:S(2)}) %copy-start.10) | copy-done | bytes 16408
  11.8 0.0 copy-start.11
  11.8 0.7 %copy-done.11 = f32[33,64]{1,0:T(8,128)S(1)} copy-done((f32[33,64]{1,0:T(8,128)S(1)}, f32[33,64]{1,0:T(8,128)}, u32[]{:S(2)}) %copy-start.11) | copy-done | bytes 8472
  12.6 0.0 copy-start.12
  12.6 0.7 %copy-done.12 = f32[2048]{0:T(1024)S(1)} copy-done((f32[2048]{0:T(1024)S(1)}, f32[2048]{0:T(1024)}, u32[]{:S(2)}) %copy-start.12) | copy-done | bytes 8216
  13.3 0.0 copy-start.13
  13.3 0.7 %copy-done.13 = bf16[3,3,128]{2,1,0:T(4,128)(2,1)S(1)} copy-done((bf16[3,3,128]{2,1,0:T(4,128)(2,1)S(1)}, bf16[3,3,128]{2,1,0:T(4,128)(2,1)}, u32[]{:S(2)}) %copy-start.13) | copy-done | bytes 2328
  14.0 0.0 copy-start.14
  14.0 0.7 %copy-done.14 = f32[3,128]{1,0:T(4,128)S(1)} copy-done((f32[3,128]{1,0:T(4,128)S(1)}, f32[3,128]{1,0:T(4,128)}, u32[]{:S(2)}) %copy-start.14) | copy-done | bytes 1560
  14.6 0.0 copy-start.15
  14.6 0.7 %copy-done.15 = f32[2,4]{1,0:T(2,128)S(1)} copy-done((f32[2,4]{1,0:T(2,128)S(1)}, f32[2,4]{1,0:T(2,128)}, u32[]{:S(2)}) %copy-start.15) | copy-done | bytes 56
  15.3 0.0 copy-start.16
  15.3 0.7 %copy-done.16 = f32[64]{0:T(128)S(1)} copy-done((f32[64]{0:T(128)S(1)}, f32[64]{0:T(128)}, u32[]{:S(2)}) %copy-start.16) | copy-done | bytes 280
  16.0 0.0 copy-start.17
  16.0 0.7 %copy-done.17 = f32[64]{0:T(128)S(1)} copy-done((f32[64]{0:T(128)S(1)}, f32[64]{0:T(128)}, u32[]{:S(2)}) %copy-start.17) | copy-done | bytes 280
  16.6 0.0 copy-start.18
  16.6 0.7 %copy-done.18 = f32[64]{0:T(128)S(1)} copy-done((f32[64]{0:T(128)S(1)}, f32[64]{0:T(128)}, u32[]{:S(2)}) %copy-start.18) | copy-done | bytes 280
  17.3 0.0 copy-start.19
  17.3 0.7 %copy-done.19 = f32[128]{0:T(128)S(1)} copy-done((f32[128]{0:T(128)S(1)}, f32[128]{0:T(128)}, u32[]{:S(2)}) %copy-start.19) | copy-done | bytes 536
  17.9 33.7 %shard_map.208 = bf16[32,2048]{1,0:T(8,128)(2,1)S(1)} custom-call(bf16[256,2048]{1,0:T(8,128)(2,1)S(1)} %copy-done.1, f32[1,2048]{1,0:T(1,128)S(1)} %bitcast.5, bf16[2048,128]{1,0:T(8,128)(2,1)S(1)} %copy-done.2, bf16[2048,128]{1,0:T(8,128)(2,1)S(1)} %copy-done.3, bf16[2048,128]{1,0:T(8,128)(2,1)S(1)} %copy-done.4, bf16[3,3,128]{2,1,0:T(4,128)(2,1)S(1)} %copy-done.13, ...), custom_call_target="tpu_custom_call" | custom-call | tf_op jit(solution)/shard_map/pallas_call | solution.py:479
  51.7 0.7 %copy.25 = bf16[32,2048]{1,0:T(8,128)(2,1)} copy(bf16[32,2048]{1,0:T(8,128)(2,1)S(1)} %shard_map.208) | data formatting | bytes 262144
Async XLA Ops:
  0.8 1.4 %copy-start = (bf16[96,8192]{1,0:T(8,128)(2,1)S(1)}, bf16[96,8192]{1,0:T(8,128)(2,1)}, u32[]{:S(2)}) copy-start(bf16[96,8192]{1,0:T(8,128)(2,1)} %constant.17.clone.feats_hbm) | copy-start | bytes 4718596
  2.2 1.2 %copy-start.1 = (bf16[256,2048]{1,0:T(8,128)(2,1)S(1)}, bf16[256,2048]{1,0:T(8,128)(2,1)}, u32[]{:S(2)}) copy-start(bf16[256,2048]{1,0:T(8,128)(2,1)} %tokens_hbm.1) | copy-start | bytes 3145732
  3.4 1.0 %copy-start.2 = (bf16[2048,128]{1,0:T(8,128)(2,1)S(1)}, bf16[2048,128]{1,0:T(8,128)(2,1)}, u32[]{:S(2)}) copy-start(bf16[2048,128]{1,0:T(8,128)(2,1)} %gate0_hbm.1) | copy-start | bytes 1572868
  4.5 1.0 %copy-start.3 = (bf16[2048,128]{1,0:T(8,128)(2,1)S(1)}, bf16[2048,128]{1,0:T(8,128)(2,1)}, u32[]{:S(2)}) copy-start(bf16[2048,128]{1,0:T(8,128)(2,1)} %gate1_hbm.1) | copy-start | bytes 1572868
  5.5 1.0 %copy-start.4 = (bf16[2048,128]{1,0:T(8,128)(2,1)S(1)}, bf16[2048,128]{1,0:T(8,128)(2,1)}, u32[]{:S(2)}) copy-start(bf16[2048,128]{1,0:T(8,128)(2,1)} %gate2_hbm.1) | copy-start | bytes 1572868
  6.6 0.9 %copy-start.5 = (bf16[2,256,256]{2,1,0:T(8,128)(2,1)S(1)}, bf16[2,256,256]{2,1,0:T(8,128)(2,1)}, u32[]{:S(2)}) copy-start(bf16[2,256,256]{2,1,0:T(8,128)(2,1)} %constant.15.clone.back_hbm) | copy-start | bytes 786436
  7.5 0.9 %copy-start.6 = (bf16[2,256,256]{2,1,0:T(8,128)(2,1)S(1)}, bf16[2,256,256]{2,1,0:T(8,128)(2,1)}, u32[]{:S(2)}) copy-start(bf16[2,256,256]{2,1,0:T(8,128)(2,1)} %constant.14.clone.second_hbm) | copy-start | bytes 786436
  8.5 0.9 %copy-start.7 = (f32[72,256]{1,0:T(8,128)S(1)}, f32[72,256]{1,0:T(8,128)}, u32[]{:S(2)}) copy-start(f32[72,256]{1,0:T(8,128)} %constant.13.clone.twiddle_hbm) | copy-start | bytes 221188
  9.4 0.9 %copy-start.8 = (bf16[144,192]{1,0:T(8,128)(2,1)S(1)}, bf16[144,192]{1,0:T(8,128)(2,1)}, u32[]{:S(2)}) copy-start(bf16[144,192]{1,0:T(8,128)(2,1)} %constant.12.clone.first_hbm) | copy-start | bytes 165892
  10.2 0.8 %copy-start.9 = (bf16[64,432]{1,0:T(8,128)(2,1)S(1)}, bf16[64,432]{1,0:T(8,128)(2,1)}, u32[]{:S(2)}) copy-start(bf16[64,432]{1,0:T(8,128)(2,1)} %constant.16.clone.last_hbm) | copy-start | bytes 165892
  11.1 0.8 %copy-start.10 = (f32[64,64]{1,0:T(8,128)S(1)}, f32[64,64]{1,0:T(8,128)}, u32[]{:S(2)}) copy-start(f32[64,64]{1,0:T(8,128)} %inner_w_hbm.1) | copy-start | bytes 49156
  11.8 0.7 %copy-start.11 = (f32[33,64]{1,0:T(8,128)S(1)}, f32[33,64]{1,0:T(8,128)}, u32[]{:S(2)}) copy-start(f32[33,64]{1,0:T(8,128)} %embed_w_hbm.1) | copy-start | bytes 25348
  12.6 0.7 %copy-start.12 = (f32[2048]{0:T(1024)S(1)}, f32[2048]{0:T(1024)}, u32[]{:S(2)}) copy-start(f32[2048]{0:T(1024)} %param.23) | copy-start | bytes 24580
  13.3 0.7 %copy-start.13 = (bf16[3,3,128]{2,1,0:T(4,128)(2,1)S(1)}, bf16[3,3,128]{2,1,0:T(4,128)(2,1)}, u32[]{:S(2)}) copy-start(bf16[3,3,128]{2,1,0:T(4,128)(2,1)} %short_w_hbm.1) | copy-start | bytes 6916
  14.0 0.7 %copy-start.14 = (f32[3,128]{1,0:T(4,128)S(1)}, f32[3,128]{1,0:T(4,128)}, u32[]{:S(2)}) copy-start(f32[3,128]{1,0:T(4,128)} %short_b_hbm.1) | copy-start | bytes 4612
  14.6 0.7 %copy-start.15 = (f32[2,4]{1,0:T(2,128)S(1)}, f32[2,4]{1,0:T(2,128)}, u32[]{:S(2)}) copy-start(f32[2,4]{1,0:T(2,128)} %skip_hbm.1) | copy-start | bytes 100
  15.3 0.7 %copy-start.16 = (f32[64]{0:T(128)S(1)}, f32[64]{0:T(128)}, u32[]{:S(2)}) copy-start(f32[64]{0:T(128)} %param.30) | copy-start | bytes 772
  16.0 0.7 %copy-start.17 = (f32[64]{0:T(128)S(1)}, f32[64]{0:T(128)}, u32[]{:S(2)}) copy-start(f32[64]{0:T(128)} %param.32) | copy-start | bytes 772
  16.6 0.7 %copy-start.18 = (f32[64]{0:T(128)S(1)}, f32[64]{0:T(128)}, u32[]{:S(2)}) copy-start(f32[64]{0:T(128)} %param.33) | copy-start | bytes 772
  17.3 0.7 %copy-start.19 = (f32[128]{0:T(128)S(1)}, f32[128]{0:T(128)}, u32[]{:S(2)}) copy-start(f32[128]{0:T(128)} %param.36) | copy-start | bytes 1540

commit v2 on v1

--- a/solution.py
+++ b/solution.py
@@ -265,14 +265,13 @@
     params[33:34, 0:64] = embed_b[...] * scale - 0.25
     params[48:49, 0:64] = inner_b[...] * scale - 0.25
     params[64:128, 0:64] = inner_w[...] * scale
-    params[0:64, 64:80] = jnp.concatenate(
-        [filter_w[o, e] for o in range(2) for e in range(2)], axis=1
-    )
     turned = params[...].T
     embed_t = wide(turned[0:64, 0:FEATS])
     inner_bias = turned[0:64, 48:49]
     inner_t = wide(turned[0:64, 64:128])
-    filter_t = wide(turned[64:80, 0:64])
+    filter_t = wide(
+        jnp.concatenate([filter_w[o, e] for o in range(2) for e in range(2)], axis=0)
+    )
 
     row8 = lax.broadcasted_iota(jnp.int32, (8, 1), 0)
     channel = (col * ROWS + me) * OWN + lax.rem(row8, OWN)
@@ -447,7 +446,7 @@
     operands = [
         tokens, norm_gain[None], first_gate, second_gate, value_weight, short_weight, short_bias,
         embed_weight, embed_bias[None], inner_weight, inner_bias[None], filter_freq[None],
-        filter_weight, filter_skip, output_gain[None], output_weight,
+        jnp.swapaxes(filter_weight, 2, 3), filter_skip, output_gain[None], output_weight,
     ] + [
         jnp.asarray(constants[name])
         for name in ("first", "twiddle", "second", "back", "last", "feats")
@@ -479,11 +478,11 @@
     return pl.pallas_call(
         kernel,
         out_shape=jax.ShapeDtypeStruct((32, WIDTH), BF),
-        in_specs=[pl.BlockSpec(memory_space=pl.ANY)] * len(operands),
+        in_specs=[pl.BlockSpec(memory_space=pltpu.HBM)] * len(operands),
         out_specs=pl.BlockSpec(memory_space=pltpu.VMEM),
         scratch_shapes=scratch,
         compiler_params=pltpu.CompilerParams(
-            collective_id=0, has_side_effects=True, vmem_limit_bytes=48 * 1024 * 1024
+            collective_id=0, has_side_effects=True, vmem_limit_bytes=67_043_328
         ),
     )(*operands)
 

time: 53.1 us -> 36.1 us (0.68); the launches traced: 52.3 us -> 36.1 us
  local copies, waits for them, and re-layouts: 18.6 us -> 1.57 us
  Pallas kernels: 33.7 us -> 34.5 us
    unnamed x42 -> x1, local copies, waits for them, and re-layouts: 18.6 us -> 1.57 us
    pallas_call x1, Pallas kernels: 33.7 us -> 34.5 us  [local(): pl.pallas_call(kernel, out_shape=jax.ShapeDtypeStruct((32, WIDTH), BF), i...]
where the time goes in v2:
time: 36.1 us
  Pallas kernels  34.5 us (96%)
  local copies, waits for them, and re-layouts  1.57 us (4%)
    pallas_call x1, Pallas kernels, local(): pl.pallas_call(kernel, out_shape=jax.ShapeDtypeStruct((32, WIDTH), BF), i...  34.5 us
    unnamed x1, local copies, waits for them, and re-layouts  1.57 us

profile of v2, /device:TPU:1, one launch (start us, length us, event | category | flops | bytes accessed | tf_op | source)
XLA Modules:
  0.0 36.1 jit_solution(13818410761737325629)
XLA Ops:
  0.0 34.5 %shard_map.208 = bf16[32,2048]{1,0:T(8,128)(2,1)} custom-call(bf16[256,2048]{1,0:T(8,128)(2,1)} %tokens_hbm.1, f32[1,2048]{1,0:T(1,128)} %bitcast.6, bf16[2048,128]{1,0:T(8,128)(2,1)} %gate0_hbm.1, bf16[2048,128]{1,0:T(8,128)(2,1)} %gate1_hbm.1, bf16[2048,128]{1,0:T(8,128)(2,1)} %gate2_hbm.1, bf16[3,3,128]{2,1,0:T(4,128)(2,1)} %short_w_hbm.1, ...), custom_call_target="tpu_custom_call" | custom-call | tf_op jit(solution)/shard_map/pallas_call | solution.py:478
  34.5 1.6 %copy.24 = bf16[32,2048]{1,0:T(8,128)(2,1)} copy(bf16[32,2048]{1,0:T(8,128)(2,1)} %shard_map.208) | data formatting | bytes 262144

commit v3 on v2

--- a/solution.py
+++ b/solution.py
@@ -27,6 +27,18 @@
 OWN = 4
 FEATS = 48
 CHUNK = 2048
+
+
+def farthest_first(steps):
+    return [offset for _, offset in sorted(steps, reverse=True) if any(offset)]
+
+
+FAR_ROWS = farthest_first(
+    [(min(dz, 8 - dz) + min(dx, 4 - dx), (dz, dx)) for dz in range(8) for dx in range(4)]
+)
+FAR_COLS = farthest_first(
+    [(2 * min(dy, 4 - dy) + dc, (dy, dc)) for dy in range(4) for dc in range(2)]
+)
 
 BF = jnp.bfloat16
 F32 = jnp.float32
@@ -163,20 +175,14 @@
 
     barrier = pltpu.get_barrier_semaphore()
 
-    def greet_row(k, carry):
-        pl.semaphore_signal(
-            barrier, inc=1, device_id=(lax.rem(me + k, ROWS), col), device_id_type=MESH
-        )
-        return carry
-
-    def greet_col(k, carry):
-        pl.semaphore_signal(
-            barrier, inc=1, device_id=(me, lax.rem(col + k, n_col)), device_id_type=MESH
-        )
-        return carry
-
-    lax.fori_loop(1, ROWS, greet_row, 0)
-    lax.fori_loop(1, n_col, greet_col, 0)
+    z, x = lax.div(me, 4), lax.rem(me, 4)
+    row_peers = [lax.rem(z + dz, 8) * 4 + lax.rem(x + dx, 4) for dz, dx in FAR_ROWS]
+    y, core = lax.div(col, 2), lax.rem(col, 2)
+    col_peers = [lax.rem(y + dy, 4) * 2 + lax.rem(core + dc, 2) for dy, dc in FAR_COLS]
+    for there in row_peers:
+        pl.semaphore_signal(barrier, inc=1, device_id=(there, col), device_id_type=MESH)
+    for there in col_peers:
+        pl.semaphore_signal(barrier, inc=1, device_id=(me, there), device_id_type=MESH)
 
     loads = [
         pltpu.make_async_copy(src, dst, load_sem.at[j])
@@ -235,27 +241,24 @@
                 packed[pl.ds(4 * half + i, ROWS, stride=8), :] = flat[
                     pl.ds(128 * half + i, ROWS, stride=4), :
                 ]
-        send1[:, b] = packed[...].reshape(ROWS, 8, COLS).astype(BF)
+        send1[b] = packed[...].reshape(ROWS, 8, COLS).astype(BF)
 
     pl.semaphore_wait(barrier, ROWS - 1 + n_col - 1)
 
-    def row_copy(source, target, number, k):
-        there = lax.rem(me + k, ROWS)
-        return pltpu.make_async_remote_copy(
-            src_ref=source.at[there],
-            dst_ref=target.at[me],
-            send_sem=send_sems.at[number],
-            recv_sem=recv_sems.at[number],
-            device_id=(there, col),
-            device_id_type=MESH,
-        )
-
-    def send_out(k, carry):
-        row_copy(send1, recv1, 0, k).start()
-        return carry
-
-    lax.fori_loop(1, ROWS, send_out, 0)
-    recv1[me] = send1[me]
+    def send_rows(source, target, number):
+        for there in row_peers:
+            pltpu.make_async_remote_copy(
+                src_ref=source.at[there],
+                dst_ref=target.at[me],
+                send_sem=send_sems.at[number],
+                recv_sem=recv_sems.at[number],
+                device_id=(there, col),
+                device_id_type=MESH,
+            ).start()
+        target[me] = source[me]
+
+    for b in (2, 0, 1):
+        send_rows(send1.at[b], recv1.at[b], b)
 
     for load in loads[5:15]:
         load.wait()
@@ -335,12 +338,12 @@
             target.at[pl.ds(0, ROWS - 1)], target.at[pl.ds(0, ROWS - 1)], recv_sems.at[number]
         ).wait()
 
-    wait_row(recv1, 0)
     row = lax.broadcasted_iota(jnp.int32, (256, COLS), 0)
     lane = lax.broadcasted_iota(jnp.int32, (256, COLS), 1)
-    smoothed = []
-    for b in range(3):
-        here = recv1[:, b].astype(F32).reshape(256, COLS)
+
+    def smoothed(b):
+        wait_row(recv1.at[b], b)
+        here = recv1[b].astype(F32).reshape(256, COLS)
         before = pltpu.roll(here, 1, axis=1)
         before = jnp.where(lane == 0, pltpu.roll(before, OWN, axis=0), before)
         before = jnp.where((lane == 0) & (row < OWN), 0.0, before)
@@ -353,13 +356,11 @@
         value = value + here.reshape(shape) * tap[1]
         value = value + after.reshape(shape) * tap[2]
         smooth[b] = value.reshape(256, COLS)
-        smoothed.append(
-            jnp.concatenate(
-                [smooth[b, pl.ds(i, LIVE, stride=OWN), :] for i in range(OWN)], axis=1
-            )
+        return jnp.concatenate(
+            [smooth[b, pl.ds(i, LIVE, stride=OWN), :] for i in range(OWN)], axis=1
         )
 
-    signal = smoothed[2]
+    signal = smoothed(2)
     for o in range(2):
         spectrum = dot_table(into_spectrum(signal, first, twiddle), second, 0, 2 * COLS)
         real, imag = spectrum[:, :COLS], spectrum[:, COLS:]
@@ -375,7 +376,8 @@
             ],
             axis=1,
         )
-        signal = smoothed[o] * (from_spectrum(product, back, last, twiddle) + direct)
+        signal = from_spectrum(product, back, last, twiddle) + direct
+        signal = signal * smoothed(o)
 
     for i in range(OWN):
         flat[pl.ds(i * LIVE, LIVE), :] = signal[:, i * COLS : (i + 1) * COLS]
@@ -386,13 +388,8 @@
             ]
     send2[...] = packed[...].reshape(ROWS, 8, COLS).astype(BF)
 
-    def send_back(k, carry):
-        row_copy(send2, recv2, 1, k).start()
-        return carry
-
-    lax.fori_loop(1, ROWS, send_back, 0)
-    recv2[me] = send2[me]
-    wait_row(recv2, 1)
+    send_rows(send2, recv2, 3)
+    wait_row(recv2, 3)
 
     values = recv2[...].astype(F32)
     squares = jnp.sum(values * values, axis=0)
@@ -404,23 +401,19 @@
         turned = flat[pl.ds(half, COLS, stride=2), :].T * out_gain[...]
         send3[4 * half : 4 * half + 4] = turned.reshape(4, 32, COLS).astype(BF)
 
-    def send_over(k, carry):
-        there = lax.rem(col + k, n_col)
+    for there in col_peers:
         pltpu.make_async_remote_copy(
             src_ref=send3.at[there],
             dst_ref=recv3.at[col],
-            send_sem=send_sems.at[2],
-            recv_sem=recv_sems.at[2],
+            send_sem=send_sems.at[4],
+            recv_sem=recv_sems.at[4],
             device_id=(me, there),
             device_id_type=MESH,
         ).start()
-        return carry
-
-    lax.fori_loop(1, n_col, send_over, 0)
     recv3[col] = send3[col]
     loads[21].wait()
     pltpu.make_async_copy(
-        recv3.at[pl.ds(0, n_col - 1)], recv3.at[pl.ds(0, n_col - 1)], recv_sems.at[2]
+        recv3.at[pl.ds(0, n_col - 1)], recv3.at[pl.ds(0, n_col - 1)], recv_sems.at[4]
     ).wait()
     mixed = jnp.concatenate([recv3[c] for c in range(n_col)], axis=1)
     for q in range(4):
@@ -428,12 +421,13 @@
             BF
         )
 
-    for number, source in ((0, send1), (1, send2)):
+    for number in range(4):
+        source = send1.at[number] if number < 3 else send2
         pltpu.make_async_copy(
             source.at[pl.ds(0, ROWS - 1)], source.at[pl.ds(0, ROWS - 1)], send_sems.at[number]
         ).wait()
     pltpu.make_async_copy(
-        send3.at[pl.ds(0, n_col - 1)], send3.at[pl.ds(0, n_col - 1)], send_sems.at[2]
+        send3.at[pl.ds(0, n_col - 1)], send3.at[pl.ds(0, n_col - 1)], send_sems.at[4]
     ).wait()
 
 
@@ -461,8 +455,8 @@
         vmem((256, WIDTH), BF),
         vmem((256, COLS), F32),
         vmem((256, COLS), F32),
-        vmem((ROWS, 3, 8, COLS), BF),
-        vmem((ROWS, 3, 8, COLS), BF),
+        vmem((3, ROWS, 8, COLS), BF),
+        vmem((3, ROWS, 8, COLS), BF),
         vmem((128, 128), F32),
         vmem((2 * LIVE * 8, COLS), F32),
         vmem((2, OWN * HALF, 2 * COLS), F32),
@@ -472,17 +466,17 @@
         vmem((8, 32, COLS), BF),
         vmem((8, 32, COLS), BF),
         pltpu.SemaphoreType.DMA((22,)),
-        pltpu.SemaphoreType.DMA((3,)),
-        pltpu.SemaphoreType.DMA((3,)),
+        pltpu.SemaphoreType.DMA((5,)),
+        pltpu.SemaphoreType.DMA((5,)),
     ]
     return pl.pallas_call(
         kernel,
-        out_shape=jax.ShapeDtypeStruct((32, WIDTH), BF),
+        out_shape=pltpu.VMEM((32, WIDTH), BF),
         in_specs=[pl.BlockSpec(memory_space=pltpu.HBM)] * len(operands),
         out_specs=pl.BlockSpec(memory_space=pltpu.VMEM),
         scratch_shapes=scratch,
         compiler_params=pltpu.CompilerParams(
-            collective_id=0, has_side_effects=True, vmem_limit_bytes=67_043_328
+            collective_id=0, has_side_effects=True, vmem_limit_bytes=66_912_256
         ),
     )(*operands)
 

time: 36.1 us -> 31.5 us (0.87)
  Pallas kernels: 34.5 us -> 30.8 us
  local copies, waits for them, and re-layouts: 1.57 us -> 0.66 us
    pallas_call x1, Pallas kernels: 34.5 us -> 30.8 us  [local(): pl.pallas_call(kernel, out_shape=pltpu.VMEM((32, WIDTH), BF), in_specs=[p...]
    unnamed x1, local copies, waits for them, and re-layouts: 1.57 us -> 0.66 us
where the time goes in v3:
time: 31.5 us
  Pallas kernels  30.8 us (98%)
  local copies, waits for them, and re-layouts  0.66 us (2%)
    pallas_call x1, Pallas kernels, local(): pl.pallas_call(kernel, out_shape=pltpu.VMEM((32, WIDTH), BF), in_specs=[p...  30.8 us
    unnamed x1, local copies, waits for them, and re-layouts  0.66 us

profile of v3, /device:TPU:1, one launch (start us, length us, event | category | flops | bytes accessed | tf_op | source)
XLA Modules:
  0.0 31.5 jit_solution(6750769003127618527)
XLA Ops:
  0.0 30.8 %shard_map.208 = bf16[32,2048]{1,0:T(8,128)(2,1)S(1)} custom-call(bf16[256,2048]{1,0:T(8,128)(2,1)} %tokens_hbm.1, f32[1,2048]{1,0:T(1,128)} %bitcast.6, bf16[2048,128]{1,0:T(8,128)(2,1)} %gate0_hbm.1, bf16[2048,128]{1,0:T(8,128)(2,1)} %gate1_hbm.1, bf16[2048,128]{1,0:T(8,128)(2,1)} %gate2_hbm.1, bf16[3,3,128]{2,1,0:T(4,128)(2,1)} %short_w_hbm.1, ...), custom_call_target="tpu_custom_call" | custom-call | tf_op jit(solution)/shard_map/pallas_call | solution.py:472
  30.8 0.7 %copy.24 = bf16[32,2048]{1,0:T(8,128)(2,1)} copy(bf16[32,2048]{1,0:T(8,128)(2,1)S(1)} %shard_map.208) | data formatting | bytes 262144

commit v4 on v3

--- a/solution.py
+++ b/solution.py
@@ -128,9 +128,7 @@
 
 def dot_table(value, table, lo, hi):
     high, low = split(value)
-    return (
-        dot(high, table[0, :, lo:hi]) + dot(low, table[0, :, lo:hi]) + dot(high, table[1, :, lo:hi])
-    )
+    return dot(high, table[0, :, lo:hi])
 
 
 def into_spectrum(signal, first, twiddle):
@@ -167,7 +165,7 @@
     tokens, norm_gain, gates, short_w, short_b, embed_w, embed_b, inner_w, inner_b, freq,
     filter_w, skip, out_gain, out_w, first, twiddle, second, back, last, feats,
     normed, flat, packed, send1, recv1, params, mixed_taps, spectra, smooth,
-    send2, recv2, send3, recv3, load_sem, send_sems, recv_sems,
+    send2, recv2, send3, recv3, gate_own, edge_out, edge_in, total, load_sem, send_sems, recv_sems,
 ):
     me = lax.axis_index("row")
     col = lax.axis_index("col")
@@ -230,12 +228,14 @@
     for load in loads[2:5]:
         load.wait()
     projected = dot(normed[...], gates[...])
-    projected = projected.astype(BF).astype(F32).T
-    for b in range(3):
+    projected = projected.astype(BF).astype(F32)
+    gate_own[...] = projected[:, 128:256]
+    edge_out[0] = projected[248:256, 128:256].astype(BF)
+    edge_out[1] = projected[0:8, 128:256].astype(BF)
+    for b in range(2):
+        turned = projected[:, b * 256 : b * 256 + 128].T
         for half in range(2):
-            flat[pl.ds(half * 128, 128), :] = projected[
-                b * 128 : (b + 1) * 128, half * 128 : (half + 1) * 128
-            ]
+            flat[pl.ds(half * 128, 128), :] = turned[:, half * 128 : (half + 1) * 128]
         for half in range(2):
             for i in range(OWN):
                 packed[pl.ds(4 * half + i, ROWS, stride=8), :] = flat[
@@ -257,8 +257,17 @@
             ).start()
         target[me] = source[me]
 
-    for b in (2, 0, 1):
-        send_rows(send1.at[b], recv1.at[b], b)
+    send_rows(send1.at[1], recv1.at[1], 2)
+    send_rows(send1.at[0], recv1.at[0], 0)
+    for side, there in ((0, lax.rem(me + 1, ROWS)), (1, lax.rem(me + ROWS - 1, ROWS))):
+        pltpu.make_async_remote_copy(
+            src_ref=edge_out.at[side],
+            dst_ref=edge_in.at[side],
+            send_sem=send_sems.at[1],
+            recv_sem=recv_sems.at[1],
+            device_id=(there, col),
+            device_id_type=MESH,
+        ).start()
 
     for load in loads[5:15]:
         load.wait()
@@ -330,7 +339,7 @@
     all_short = short_w[...].astype(F32)
     columns = [
         [own_column(all_short[b, j : j + 1]) for j in range(3)] + [own_column(short_b[b : b + 1, :])]
-        for b in range(3)
+        for b in (0, 2)
     ]
 
     def wait_row(target, number):
@@ -342,7 +351,7 @@
     lane = lax.broadcasted_iota(jnp.int32, (256, COLS), 1)
 
     def smoothed(b):
-        wait_row(recv1.at[b], b)
+        wait_row(recv1.at[b], 2 * b)
         here = recv1[b].astype(F32).reshape(256, COLS)
         before = pltpu.roll(here, 1, axis=1)
         before = jnp.where(lane == 0, pltpu.roll(before, OWN, axis=0), before)
@@ -360,7 +369,7 @@
             [smooth[b, pl.ds(i, LIVE, stride=OWN), :] for i in range(OWN)], axis=1
         )
 
-    signal = smoothed(2)
+    signal = smoothed(1)
     for o in range(2):
         spectrum = dot_table(into_spectrum(signal, first, twiddle), second, 0, 2 * COLS)
         real, imag = spectrum[:, :COLS], spectrum[:, COLS:]
@@ -377,7 +386,8 @@
             axis=1,
         )
         signal = from_spectrum(product, back, last, twiddle) + direct
-        signal = signal * smoothed(o)
+        if o == 0:
+            signal = signal * smoothed(0)
 
     for i in range(OWN):
         flat[pl.ds(i * LIVE, LIVE), :] = signal[:, i * COLS : (i + 1) * COLS]
@@ -389,43 +399,57 @@
     send2[...] = packed[...].reshape(ROWS, 8, COLS).astype(BF)
 
     send_rows(send2, recv2, 3)
+    pltpu.make_async_copy(edge_in, edge_in, recv_sems.at[1]).wait()
+    position = lax.broadcasted_iota(jnp.int32, (256, COLS), 0)
+    here = gate_own[...]
+    first_edge = edge_in[0].astype(F32)[7:8] * jnp.where(me == 0, 0.0, 1.0)
+    last_edge = edge_in[1].astype(F32)[0:1] * jnp.where(me == ROWS - 1, 0.0, 1.0)
+    before = jnp.where(position == 0, first_edge, pltpu.roll(here, 1, axis=0))
+    after = jnp.where(position == 255, last_edge, pltpu.roll(here, 255, axis=0))
+    value = short_b[1:2, :] + before * all_short[1, 0:1]
+    value = value + here * all_short[1, 1:2]
+    gate_own[...] = value + after * all_short[1, 2:3]
+
     wait_row(recv2, 3)
 
-    values = recv2[...].astype(F32)
-    squares = jnp.sum(values * values, axis=0)
-    squares = squares + pltpu.roll(squares, 4, axis=0)
-    squares = squares + pltpu.roll(squares, 2, axis=0)
-    factor = lax.rsqrt(squares * (GROUPS / CHANNELS) + NORM_EPS)
-    flat[...] = (values * factor[None]).reshape(256, COLS)
+    flat[...] = recv2[...].astype(F32).reshape(256, COLS)
     for half in range(2):
-        turned = flat[pl.ds(half, COLS, stride=2), :].T * out_gain[...]
-        send3[4 * half : 4 * half + 4] = turned.reshape(4, 32, COLS).astype(BF)
-
-    for there in col_peers:
+        gated = flat[pl.ds(half, COLS, stride=2), :].T * gate_own[half * 128 : half * 128 + 128]
+        mean = jnp.mean(gated * gated, axis=1, keepdims=True)
+        gated = gated * lax.rsqrt(mean + NORM_EPS) * out_gain[...]
+        send3[4 * half : 4 * half + 4] = gated.reshape(4, 32, COLS).astype(BF)
+
+    for (dy, _), there in zip(FAR_COLS, col_peers):
         pltpu.make_async_remote_copy(
             src_ref=send3.at[there],
             dst_ref=recv3.at[col],
             send_sem=send_sems.at[4],
-            recv_sem=recv_sems.at[4],
+            recv_sem=recv_sems.at[4 + dy],
             device_id=(me, there),
             device_id_type=MESH,
         ).start()
     recv3[col] = send3[col]
     loads[21].wait()
-    pltpu.make_async_copy(
-        recv3.at[pl.ds(0, n_col - 1)], recv3.at[pl.ds(0, n_col - 1)], recv_sems.at[4]
-    ).wait()
-    mixed = jnp.concatenate([recv3[c] for c in range(n_col)], axis=1)
-    for q in range(4):
-        out_ref[:, q * 512 : (q + 1) * 512] = dot(mixed, out_w[:, q * 512 : (q + 1) * 512]).astype(
-            BF
-        )
-
-    for number in range(4):
-        source = send1.at[number] if number < 3 else send2
+    for dy in (0, 1, 3, 2):
+        count = 2 if dy else 1
+        pltpu.make_async_copy(
+            recv3.at[pl.ds(0, count)], recv3.at[pl.ds(0, count)], recv_sems.at[4 + dy]
+        ).wait()
+        source = lax.rem(y + 4 - dy, 4)
+        mixed = jnp.concatenate([recv3[2 * source], recv3[2 * source + 1]], axis=1)
+        part = dot(mixed, out_w[pl.ds(pl.multiple_of(source * 256, 256), 256), :])
+        if dy == 0:
+            total[...] = part
+        elif dy != 2:
+            total[...] += part
+        else:
+            out_ref[...] = (total[...] + part).astype(BF)
+
+    for number, source in ((2, send1.at[1]), (0, send1.at[0]), (3, send2)):
         pltpu.make_async_copy(
             source.at[pl.ds(0, ROWS - 1)], source.at[pl.ds(0, ROWS - 1)], send_sems.at[number]
         ).wait()
+    pltpu.make_async_copy(edge_out, edge_out, send_sems.at[1]).wait()
     pltpu.make_async_copy(
         send3.at[pl.ds(0, n_col - 1)], send3.at[pl.ds(0, n_col - 1)], send_sems.at[4]
     ).wait()
@@ -455,19 +479,23 @@
         vmem((256, WIDTH), BF),
         vmem((256, COLS), F32),
         vmem((256, COLS), F32),
-        vmem((3, ROWS, 8, COLS), BF),
-        vmem((3, ROWS, 8, COLS), BF),
+        vmem((2, ROWS, 8, COLS), BF),
+        vmem((2, ROWS, 8, COLS), BF),
         vmem((128, 128), F32),
         vmem((2 * LIVE * 8, COLS), F32),
         vmem((2, OWN * HALF, 2 * COLS), F32),
-        vmem((3, 256, COLS), F32),
+        vmem((2, 256, COLS), F32),
         vmem((ROWS, 8, COLS), BF),
         vmem((ROWS, 8, COLS), BF),
         vmem((8, 32, COLS), BF),
         vmem((8, 32, COLS), BF),
+        vmem((256, COLS), F32),
+        vmem((2, 8, COLS), BF),
+        vmem((2, 8, COLS), BF),
+        vmem((32, WIDTH), F32),
         pltpu.SemaphoreType.DMA((22,)),
-        pltpu.SemaphoreType.DMA((5,)),
-        pltpu.SemaphoreType.DMA((5,)),
+        pltpu.SemaphoreType.DMA((8,)),
+        pltpu.SemaphoreType.DMA((8,)),
     ]
     return pl.pallas_call(
         kernel,

time: 31.5 us -> 30.6 us (0.971)
  Pallas kernels: 30.8 us -> 29.9 us
    pallas_call x1, Pallas kernels: 30.8 us -> 29.9 us  [local(): pl.pallas_call(kernel, out_shape=pltpu.VMEM((32, WIDTH), BF), in_specs=[p...]
where the time goes in v4:
time: 30.6 us; the launch traced here: 30.5 us
  Pallas kernels  29.9 us (98%)
  local copies, waits for them, and re-layouts  0.66 us (2%)
    pallas_call x1, Pallas kernels, local(): pl.pallas_call(kernel, out_shape=pltpu.VMEM((32, WIDTH), BF), in_specs=[p...  29.9 us
    unnamed x1, local copies, waits for them, and re-layouts  0.66 us

profile of v4, /device:TPU:1, one launch (start us, length us, event | category | flops | bytes accessed | tf_op | source)
XLA Modules:
  0.0 30.5 jit_solution(11665669943817784120)
XLA Ops:
  0.0 29.9 %shard_map.208 = bf16[32,2048]{1,0:T(8,128)(2,1)S(1)} custom-call(bf16[256,2048]{1,0:T(8,128)(2,1)} %tokens_hbm.1, f32[1,2048]{1,0:T(1,128)} %bitcast.6, bf16[2048,128]{1,0:T(8,128)(2,1)} %gate0_hbm.1, bf16[2048,128]{1,0:T(8,128)(2,1)} %gate1_hbm.1, bf16[2048,128]{1,0:T(8,128)(2,1)} %gate2_hbm.1, bf16[3,3,128]{2,1,0:T(4,128)(2,1)} %short_w_hbm.1, ...), custom_call_target="tpu_custom_call" | custom-call | tf_op jit(solution)/shard_map/pallas_call | solution.py:500
  29.9 0.7 %copy.24 = bf16[32,2048]{1,0:T(8,128)(2,1)} copy(bf16[32,2048]{1,0:T(8,128)(2,1)S(1)} %shard_map.208) | data formatting | bytes 262144

commit v5 on v4

--- a/solution.py
+++ b/solution.py
@@ -132,10 +132,10 @@
 
 
 def into_spectrum(signal, first, twiddle):
-    part = dot(first[...], tall(signal))
+    part = dot(first[:,:64], signal.astype(BF))
     cos, sin = twiddle[:, :COLS], twiddle[:, COLS:]
     pieces = []
-    for i in range(OWN):
+    for i in range(signal.shape[1] // COLS):
         real = part[:HALF, i * COLS : (i + 1) * COLS]
         imag = part[HALF:, i * COLS : (i + 1) * COLS]
         pieces.append(jnp.concatenate([real * cos + imag * sin, imag * cos - real * sin], axis=1))
@@ -146,7 +146,7 @@
     part = dot_table(spectrum, back, 0, 2 * COLS)
     cos, sin = twiddle[:, :COLS], twiddle[:, COLS:]
     reals, imags = [], []
-    for i in range(OWN):
+    for i in range(spectrum.shape[0] // HALF):
         real = part[i * HALF : (i + 1) * HALF, :COLS]
         imag = part[i * HALF : (i + 1) * HALF, COLS:]
         reals.append(real * cos - imag * sin)
@@ -154,7 +154,7 @@
     turned = jnp.concatenate(
         [jnp.concatenate(reals, axis=1), jnp.concatenate(imags, axis=1)], axis=0
     )
-    return dot(last[...], tall(turned))
+    return dot(last[:,:144], turned.astype(BF))
 
 
 def kernel(
@@ -165,22 +165,11 @@
     tokens, norm_gain, gates, short_w, short_b, embed_w, embed_b, inner_w, inner_b, freq,
     filter_w, skip, out_gain, out_w, first, twiddle, second, back, last, feats,
     normed, flat, packed, send1, recv1, params, mixed_taps, spectra, smooth,
-    send2, recv2, send3, recv3, gate_own, edge_out, edge_in, total, load_sem, send_sems, recv_sems,
+    send2, recv2, send3, recv3, gate_own, gate_in, edge_out, edge_in, total, load_sem, send_sems, recv_sems,
 ):
     me = lax.axis_index("row")
     col = lax.axis_index("col")
     n_col = 8
-
-    barrier = pltpu.get_barrier_semaphore()
-
-    z, x = lax.div(me, 4), lax.rem(me, 4)
-    row_peers = [lax.rem(z + dz, 8) * 4 + lax.rem(x + dx, 4) for dz, dx in FAR_ROWS]
-    y, core = lax.div(col, 2), lax.rem(col, 2)
-    col_peers = [lax.rem(y + dy, 4) * 2 + lax.rem(core + dc, 2) for dy, dc in FAR_COLS]
-    for there in row_peers:
-        pl.semaphore_signal(barrier, inc=1, device_id=(there, col), device_id_type=MESH)
-    for there in col_peers:
-        pl.semaphore_signal(barrier, inc=1, device_id=(me, there), device_id_type=MESH)
 
     loads = [
         pltpu.make_async_copy(src, dst, load_sem.at[j])
@@ -214,6 +203,18 @@
     for load in loads:
         load.start()
 
+    barrier = pltpu.get_barrier_semaphore()
+
+    z, x = lax.div(me, 4), lax.rem(me, 4)
+    row_peers = [lax.rem(z + dz, 8) * 4 + lax.rem(x + dx, 4) for dz, dx in FAR_ROWS]
+    y, core = lax.div(col, 2), lax.rem(col, 2)
+    partner = y * 2 + 1 - core
+    col_peers = [lax.rem(y + dy, 4) * 2 + lax.rem(core + dc, 2) for dy, dc in FAR_COLS]
+    for there in row_peers:
+        pl.semaphore_signal(barrier, inc=1, device_id=(there, col), device_id_type=MESH)
+    for there in col_peers:
+        pl.semaphore_signal(barrier, inc=1, device_id=(me, there), device_id_type=MESH)
+
     for load in loads[0:2]:
         load.wait()
 
@@ -229,7 +230,7 @@
         load.wait()
     projected = dot(normed[...], gates[...])
     projected = projected.astype(BF).astype(F32)
-    gate_own[...] = projected[:, 128:256]
+    gate_own[0:256, :] = projected[:, 128:256]
     edge_out[0] = projected[248:256, 128:256].astype(BF)
     edge_out[1] = projected[0:8, 128:256].astype(BF)
     for b in range(2):
@@ -347,6 +348,26 @@
             target.at[pl.ds(0, ROWS - 1)], target.at[pl.ds(0, ROWS - 1)], recv_sems.at[number]
         ).wait()
 
+    pltpu.make_async_copy(edge_in, edge_in, recv_sems.at[1]).wait()
+    position = lax.broadcasted_iota(jnp.int32, (256, COLS), 0)
+    here = gate_own[0:256, :]
+    first_edge = edge_in[0].astype(F32)[7:8] * jnp.where(me == 0, 0.0, 1.0)
+    last_edge = edge_in[1].astype(F32)[0:1] * jnp.where(me == ROWS - 1, 0.0, 1.0)
+    before = jnp.where(position == 0, first_edge, pltpu.roll(here, 1, axis=0))
+    after = jnp.where(position == 255, last_edge, pltpu.roll(here, 255, axis=0))
+    value = short_b[1:2, :] + before * all_short[1, 0:1]
+    value = value + here * all_short[1, 1:2]
+    gate_own[0:256, :] = value + after * all_short[1, 2:3]
+    gate_own[256:264, :] = jnp.broadcast_to(out_gain[...], (8, COLS))
+    pltpu.make_async_remote_copy(
+        src_ref=gate_own,
+        dst_ref=gate_in,
+        send_sem=send_sems.at[5],
+        recv_sem=recv_sems.at[8],
+        device_id=(me, partner),
+        device_id_type=MESH,
+    ).start()
+
     row = lax.broadcasted_iota(jnp.int32, (256, COLS), 0)
     lane = lax.broadcasted_iota(jnp.int32, (256, COLS), 1)
 
@@ -369,25 +390,46 @@
             [smooth[b, pl.ds(i, LIVE, stride=OWN), :] for i in range(OWN)], axis=1
         )
 
-    signal = smoothed(1)
+    pairs = 2
+    value = smoothed(1)
+    signals = [value[:, p * COLS : (p + pairs) * COLS] for p in range(0, OWN, pairs)]
     for o in range(2):
-        spectrum = dot_table(into_spectrum(signal, first, twiddle), second, 0, 2 * COLS)
-        real, imag = spectrum[:, :COLS], spectrum[:, COLS:]
-        t_real, t_imag = spectra[o, :, :COLS], spectra[o, :, COLS:]
-        product = jnp.concatenate(
-            [real * t_real - imag * t_imag, real * t_imag + imag * t_real], axis=1
-        )
-        direct = jnp.concatenate(
-            [
-                signal[:, i * COLS : (i + 1) * COLS]
-                * jnp.broadcast_to(skip[o : o + 1, i : i + 1], (LIVE, COLS))
-                for i in range(OWN)
-            ],
-            axis=1,
-        )
-        signal = from_spectrum(product, back, last, twiddle) + direct
+        spectrum = [
+            dot_table(into_spectrum(signal, first, twiddle), second, 0, 2 * COLS)
+            for signal in signals
+        ]
+        products = []
+        for p, found in enumerate(spectrum):
+            real, imag = found[:, :COLS], found[:, COLS:]
+            rows = slice(p * pairs * HALF, (p + 1) * pairs * HALF)
+            t_real, t_imag = spectra[o, rows, :COLS], spectra[o, rows, COLS:]
+            products.append(
+                jnp.concatenate(
+                    [real * t_real - imag * t_imag, real * t_imag + imag * t_real], axis=1
+                )
+            )
+        convolved = [from_spectrum(product, back, last, twiddle) for product in products]
+        signals = [
+            found
+            + jnp.concatenate(
+                [
+                    signal[:, i * COLS : (i + 1) * COLS]
+                    * jnp.broadcast_to(
+                        skip[o : o + 1, p * pairs + i : p * pairs + i + 1], (LIVE, COLS)
+                    )
+                    for i in range(pairs)
+                ],
+                axis=1,
+            )
+            for p, (found, signal) in enumerate(zip(convolved, signals))
+        ]
         if o == 0:
-            signal = signal * smoothed(0)
+            gate = smoothed(0)
+            signals = [
+                signal * gate[:, p * pairs * COLS : (p + 1) * pairs * COLS]
+                for p, signal in enumerate(signals)
+            ]
+    signal = jnp.concatenate(signals, axis=1)
 
     for i in range(OWN):
         flat[pl.ds(i * LIVE, LIVE), :] = signal[:, i * COLS : (i + 1) * COLS]
@@ -398,37 +440,35 @@
             ]
     send2[...] = packed[...].reshape(ROWS, 8, COLS).astype(BF)
 
-    send_rows(send2, recv2, 3)
-    pltpu.make_async_copy(edge_in, edge_in, recv_sems.at[1]).wait()
-    position = lax.broadcasted_iota(jnp.int32, (256, COLS), 0)
-    here = gate_own[...]
-    first_edge = edge_in[0].astype(F32)[7:8] * jnp.where(me == 0, 0.0, 1.0)
-    last_edge = edge_in[1].astype(F32)[0:1] * jnp.where(me == ROWS - 1, 0.0, 1.0)
-    before = jnp.where(position == 0, first_edge, pltpu.roll(here, 1, axis=0))
-    after = jnp.where(position == 255, last_edge, pltpu.roll(here, 255, axis=0))
-    value = short_b[1:2, :] + before * all_short[1, 0:1]
-    value = value + here * all_short[1, 1:2]
-    gate_own[...] = value + after * all_short[1, 2:3]
-
-    wait_row(recv2, 3)
+    for there in row_peers + [me]:
+        pltpu.make_async_remote_copy(
+            src_ref=send2.at[there],
+            dst_ref=recv2.at[me],
+            send_sem=send_sems.at[3],
+            recv_sem=recv_sems.at[3],
+            device_id=(there, partner),
+            device_id_type=MESH,
+        ).start()
+    pltpu.make_async_copy(recv2, recv2, recv_sems.at[3]).wait()
+    pltpu.make_async_copy(gate_in, gate_in, recv_sems.at[8]).wait()
 
     flat[...] = recv2[...].astype(F32).reshape(256, COLS)
     for half in range(2):
-        gated = flat[pl.ds(half, COLS, stride=2), :].T * gate_own[half * 128 : half * 128 + 128]
+        gated = flat[pl.ds(half, COLS, stride=2), :].T * gate_in[half * 128 : half * 128 + 128]
         mean = jnp.mean(gated * gated, axis=1, keepdims=True)
-        gated = gated * lax.rsqrt(mean + NORM_EPS) * out_gain[...]
+        gated = gated * lax.rsqrt(mean + NORM_EPS) * gate_in[256:257]
         send3[4 * half : 4 * half + 4] = gated.reshape(4, 32, COLS).astype(BF)
 
     for (dy, _), there in zip(FAR_COLS, col_peers):
         pltpu.make_async_remote_copy(
             src_ref=send3.at[there],
-            dst_ref=recv3.at[col],
+            dst_ref=recv3.at[partner],
             send_sem=send_sems.at[4],
             recv_sem=recv_sems.at[4 + dy],
             device_id=(me, there),
             device_id_type=MESH,
         ).start()
-    recv3[col] = send3[col]
+    recv3[partner] = send3[col]
     loads[21].wait()
     for dy in (0, 1, 3, 2):
         count = 2 if dy else 1
@@ -445,11 +485,13 @@
         else:
             out_ref[...] = (total[...] + part).astype(BF)
 
-    for number, source in ((2, send1.at[1]), (0, send1.at[0]), (3, send2)):
+    for number, source in ((2, send1.at[1]), (0, send1.at[0])):
         pltpu.make_async_copy(
             source.at[pl.ds(0, ROWS - 1)], source.at[pl.ds(0, ROWS - 1)], send_sems.at[number]
         ).wait()
     pltpu.make_async_copy(edge_out, edge_out, send_sems.at[1]).wait()
+    pltpu.make_async_copy(send2, send2, send_sems.at[3]).wait()
+    pltpu.make_async_copy(gate_own, gate_own, send_sems.at[5]).wait()
     pltpu.make_async_copy(
         send3.at[pl.ds(0, n_col - 1)], send3.at[pl.ds(0, n_col - 1)], send_sems.at[4]
     ).wait()
@@ -489,13 +531,14 @@
         vmem((ROWS, 8, COLS), BF),
         vmem((8, 32, COLS), BF),
         vmem((8, 32, COLS), BF),
-        vmem((256, COLS), F32),
+        vmem((264, COLS), F32),
+        vmem((264, COLS), F32),
         vmem((2, 8, COLS), BF),
         vmem((2, 8, COLS), BF),
         vmem((32, WIDTH), F32),
         pltpu.SemaphoreType.DMA((22,)),
-        pltpu.SemaphoreType.DMA((8,)),
-        pltpu.SemaphoreType.DMA((8,)),
+        pltpu.SemaphoreType.DMA((6,)),
+        pltpu.SemaphoreType.DMA((9,)),
     ]
     return pl.pallas_call(
         kernel,

time: 30.6 us -> 29.8 us (0.974)
  Pallas kernels: 29.9 us -> 29.1 us
    pallas_call x1, Pallas kernels: 29.9 us -> 29.1 us  [local(): pl.pallas_call(kernel, out_shape=pltpu.VMEM((32, WIDTH), BF), in_specs=[p...]
where the time goes in v5:
time: 29.8 us; the launch traced here: 29.7 us
  Pallas kernels  29.1 us (98%)
  local copies, waits for them, and re-layouts  0.66 us (2%)
    pallas_call x1, Pallas kernels, local(): pl.pallas_call(kernel, out_shape=pltpu.VMEM((32, WIDTH), BF), in_specs=[p...  29.1 us
    unnamed x1, local copies, waits for them, and re-layouts  0.66 us

profile of v5, /device:TPU:1, one launch (start us, length us, event | category | flops | bytes accessed | tf_op | source)
XLA Modules:
  0.0 29.7 jit_solution(2331972764087015194)
XLA Ops:
  0.0 29.1 %shard_map.208 = bf16[32,2048]{1,0:T(8,128)(2,1)S(1)} custom-call(bf16[256,2048]{1,0:T(8,128)(2,1)} %tokens_hbm.1, f32[1,2048]{1,0:T(1,128)} %bitcast.6, bf16[2048,128]{1,0:T(8,128)(2,1)} %gate0_hbm.1, bf16[2048,128]{1,0:T(8,128)(2,1)} %gate1_hbm.1, bf16[2048,128]{1,0:T(8,128)(2,1)} %gate2_hbm.1, bf16[3,3,128]{2,1,0:T(4,128)(2,1)} %short_w_hbm.1, ...), custom_call_target="tpu_custom_call" | custom-call | tf_op jit(solution)/shard_map/pallas_call | solution.py:543
  29.1 0.7 %copy.24 = bf16[32,2048]{1,0:T(8,128)(2,1)} copy(bf16[32,2048]{1,0:T(8,128)(2,1)S(1)} %shard_map.208) | data formatting | bytes 262144

commit v6 on v5

--- a/solution.py
+++ b/solution.py
@@ -21,6 +21,7 @@
 WIDTH = 2048
 COLS = 128
 LIVE = 64
+EAGER = 1
 HALF = 72
 TOTAL = 16384
 ROWS = 32
@@ -66,8 +67,11 @@
     back = np.block([[cos_out, sin_out], [-sin_out, cos_out]])
     weight = np.where((k1 == 0) | (k1 == COLS // 2), 1.0, 2.0) * (k1 <= COLS // 2)
     last = np.concatenate([cos_in.T * weight, -sin_in.T * weight], 1) / TOTAL
-    first_h, first_l = split_np(first)
-    last_h, last_l = split_np(last)
+    tables = np.zeros((720, 2 * COLS))
+    tables[0:256] = second
+    tables[256:512] = back
+    tables[512 : 512 + 2 * HALF, :LIVE] = first
+    tables[656:720, : 2 * HALF] = last
     n = np.arange(LENGTH)
     ramp = np.linspace(0.0, 1.0, LENGTH)[None, :]
     bands = np.linspace(0.0001, FREQ_BANDS - 1, FREQ_BANDS, dtype=np.float32).astype(np.float64)
@@ -78,11 +82,8 @@
     feats[1 + FREQ_BANDS : 1 + 2 * FREQ_BANDS] = -np.sin(angle)
     feats[1 + 2 * FREQ_BANDS] = 1.0
     return dict(
-        first=np.concatenate([first_h, first_l, first_h], 1),
         twiddle=twiddle,
-        second=np.stack(split_np(second)),
-        back=np.stack(split_np(back)),
-        last=np.concatenate([last_h, last_l, last_h], 1),
+        tables=split_np(tables)[0],
         feats=np.concatenate(split_np(feats), 0),
     )
 
@@ -126,24 +127,19 @@
     return jnp.concatenate([high, low, high], axis=1)
 
 
-def dot_table(value, table, lo, hi):
-    high, low = split(value)
-    return dot(high, table[0, :, lo:hi])
-
-
-def into_spectrum(signal, first, twiddle):
-    part = dot(first[:,:64], signal.astype(BF))
+def into_spectrum(signal, tables, twiddle):
+    part = dot(tables[512:656, :LIVE], signal.astype(BF))
     cos, sin = twiddle[:, :COLS], twiddle[:, COLS:]
     pieces = []
     for i in range(signal.shape[1] // COLS):
         real = part[:HALF, i * COLS : (i + 1) * COLS]
         imag = part[HALF:, i * COLS : (i + 1) * COLS]
         pieces.append(jnp.concatenate([real * cos + imag * sin, imag * cos - real * sin], axis=1))
-    return jnp.concatenate(pieces, axis=0)
-
-
-def from_spectrum(spectrum, back, last, twiddle):
-    part = dot_table(spectrum, back, 0, 2 * COLS)
+    return jnp.concatenate(pieces, axis=0).astype(BF)
+
+
+def from_spectrum(spectrum, tables, twiddle):
+    part = dot(spectrum.astype(BF), tables[256:512, :])
     cos, sin = twiddle[:, :COLS], twiddle[:, COLS:]
     reals, imags = [], []
     for i in range(spectrum.shape[0] // HALF):
@@ -154,16 +150,16 @@
     turned = jnp.concatenate(
         [jnp.concatenate(reals, axis=1), jnp.concatenate(imags, axis=1)], axis=0
     )
-    return dot(last[:,:144], turned.astype(BF))
+    return dot(tables[656:720, : 2 * HALF], turned.astype(BF))
 
 
 def kernel(
     tokens_hbm, norm_gain_hbm, gate0_hbm, gate1_hbm, gate2_hbm, short_w_hbm, short_b_hbm,
     embed_w_hbm, embed_b_hbm, inner_w_hbm, inner_b_hbm, freq_hbm, filter_w_hbm, skip_hbm,
-    out_gain_hbm, out_w_hbm, first_hbm, twiddle_hbm, second_hbm, back_hbm, last_hbm, feats_hbm,
+    out_gain_hbm, out_w_hbm, twiddle_hbm, tables_hbm, feats_hbm,
     out_ref,
-    tokens, norm_gain, gates, short_w, short_b, embed_w, embed_b, inner_w, inner_b, freq,
-    filter_w, skip, out_gain, out_w, first, twiddle, second, back, last, feats,
+    tokens, norm_gain, gates, short_w, short_b, embed_w, lines, inner_w,
+    filter_w, skip, out_gain, out_w, twiddle, tables, feats,
     normed, flat, packed, send1, recv1, params, mixed_taps, spectra, smooth,
     send2, recv2, send3, recv3, gate_own, gate_in, edge_out, edge_in, total, load_sem, send_sems, recv_sems,
 ):
@@ -171,37 +167,33 @@
     col = lax.axis_index("col")
     n_col = 8
 
-    loads = [
-        pltpu.make_async_copy(src, dst, load_sem.at[j])
-        for j, (src, dst) in enumerate(
-            [
-                (tokens_hbm, tokens),
-                (norm_gain_hbm, norm_gain),
-                (gate0_hbm, gates.at[:, 0:128]),
-                (gate1_hbm, gates.at[:, 128:256]),
-                (gate2_hbm, gates.at[:, 256:384]),
-                (embed_w_hbm, embed_w),
-                (embed_b_hbm, embed_b),
-                (inner_w_hbm, inner_w),
-                (inner_b_hbm, inner_b),
-                (freq_hbm, freq),
-                (filter_w_hbm, filter_w),
-                (feats_hbm, feats),
-                (first_hbm, first),
-                (twiddle_hbm, twiddle),
-                (second_hbm, second),
-                (short_w_hbm, short_w),
-                (short_b_hbm, short_b),
-                (skip_hbm, skip),
-                (back_hbm, back),
-                (last_hbm, last),
-                (out_gain_hbm, out_gain),
-                (out_w_hbm, out_w),
-            ]
-        )
+    copies = [
+        (tokens_hbm, tokens, 0),
+        (norm_gain_hbm, norm_gain, 1),
+        (gate0_hbm, gates.at[:, 0:128], 2),
+        (gate1_hbm, gates.at[:, 128:256], 2),
+        (gate2_hbm, gates.at[:, 256:384], 2),
+        (embed_w_hbm, embed_w, 3),
+        (embed_b_hbm, lines.at[0], 4),
+        (inner_b_hbm, lines.at[1], 4),
+        (freq_hbm, lines.at[2], 4),
+        (inner_w_hbm, inner_w, 5),
+        (filter_w_hbm, filter_w, 6),
+        (feats_hbm, feats, 7),
+        (tables_hbm, tables, 8),
+        (twiddle_hbm, twiddle, 9),
+        (short_w_hbm, short_w, 10),
+        (short_b_hbm, short_b, 11),
+        (skip_hbm, skip, 12),
+        (out_gain_hbm, out_gain, 13),
+        (out_w_hbm, out_w, 14),
     ]
-    for load in loads:
-        load.start()
+    for source, target, number in copies:
+        pltpu.make_async_copy(source, target, load_sem.at[number]).start()
+
+    def loaded(*targets):
+        for target, number in targets:
+            pltpu.make_async_copy(target, target, load_sem.at[number]).wait()
 
     barrier = pltpu.get_barrier_semaphore()
 
@@ -215,8 +207,7 @@
     for there in col_peers:
         pl.semaphore_signal(barrier, inc=1, device_id=(me, there), device_id_type=MESH)
 
-    for load in loads[0:2]:
-        load.wait()
+    loaded((tokens, 0), (norm_gain, 1))
 
     def normalise(j, carry):
         rows = pl.ds(pl.multiple_of(j * 64, 64), 64)
@@ -226,8 +217,7 @@
         return carry
 
     lax.fori_loop(0, 4, normalise, 0)
-    for load in loads[2:5]:
-        load.wait()
+    loaded((gates, 2))
     projected = dot(normed[...], gates[...])
     projected = projected.astype(BF).astype(F32)
     gate_own[0:256, :] = projected[:, 128:256]
@@ -251,7 +241,7 @@
             pltpu.make_async_remote_copy(
                 src_ref=source.at[there],
                 dst_ref=target.at[me],
-                send_sem=send_sems.at[number],
+                send_sem=send_sems.at[0],
                 recv_sem=recv_sems.at[number],
                 device_id=(there, col),
                 device_id_type=MESH,
@@ -270,13 +260,13 @@
             device_id_type=MESH,
         ).start()
 
-    for load in loads[5:15]:
-        load.wait()
+    loaded((embed_w, 3), (lines, 4), (inner_w, 5), (filter_w, 6), (feats, 7), (tables, 8))
+    loaded((twiddle, 9))
     params[...] = jnp.zeros_like(params)
-    scale = freq[...] * (1.0 / (2.0 * math.pi))
+    scale = lines[2] * (1.0 / (2.0 * math.pi))
     params[0:33, 0:64] = embed_w[...] * scale
-    params[33:34, 0:64] = embed_b[...] * scale - 0.25
-    params[48:49, 0:64] = inner_b[...] * scale - 0.25
+    params[33:34, 0:64] = lines[0] * scale - 0.25
+    params[48:49, 0:64] = lines[1] * scale - 0.25
     params[64:128, 0:64] = inner_w[...] * scale
     turned = params[...].T
     embed_t = wide(turned[0:64, 0:FEATS])
@@ -323,12 +313,12 @@
                 ],
                 axis=1,
             )
-            spectra[o, :, part * COLS : (part + 1) * COLS] = dot_table(
-                into_spectrum(signal, first, twiddle), second, part * COLS, (part + 1) * COLS
+            spectra[o, :, part * COLS : (part + 1) * COLS] = dot(
+                into_spectrum(signal, tables, twiddle),
+                tables[0:256, part * COLS : (part + 1) * COLS],
             )
 
-    for load in loads[15:21]:
-        load.wait()
+    loaded((short_w, 10), (short_b, 11), (skip, 12), (out_gain, 13))
     lane8 = lax.broadcasted_iota(jnp.int32, (8, COLS), 1)
     mine = lane8 == OWN * me + lax.rem(lax.broadcasted_iota(jnp.int32, (8, COLS), 0), OWN)
 
@@ -362,7 +352,7 @@
     pltpu.make_async_remote_copy(
         src_ref=gate_own,
         dst_ref=gate_in,
-        send_sem=send_sems.at[5],
+        send_sem=send_sems.at[4],
         recv_sem=recv_sems.at[8],
         device_id=(me, partner),
         device_id_type=MESH,
@@ -395,7 +385,7 @@
     signals = [value[:, p * COLS : (p + pairs) * COLS] for p in range(0, OWN, pairs)]
     for o in range(2):
         spectrum = [
-            dot_table(into_spectrum(signal, first, twiddle), second, 0, 2 * COLS)
+            dot(into_spectrum(signal, tables, twiddle), tables[0:256, :])
             for signal in signals
         ]
         products = []
@@ -408,7 +398,7 @@
                     [real * t_real - imag * t_imag, real * t_imag + imag * t_real], axis=1
                 )
             )
-        convolved = [from_spectrum(product, back, last, twiddle) for product in products]
+        convolved = [from_spectrum(product, tables, twiddle) for product in products]
         signals = [
             found
             + jnp.concatenate(
@@ -444,7 +434,7 @@
         pltpu.make_async_remote_copy(
             src_ref=send2.at[there],
             dst_ref=recv2.at[me],
-            send_sem=send_sems.at[3],
+            send_sem=send_sems.at[2],
             recv_sem=recv_sems.at[3],
             device_id=(there, partner),
             device_id_type=MESH,
@@ -452,25 +442,30 @@
     pltpu.make_async_copy(recv2, recv2, recv_sems.at[3]).wait()
     pltpu.make_async_copy(gate_in, gate_in, recv_sems.at[8]).wait()
 
+    def send_over(there, dy):
+        pltpu.make_async_remote_copy(
+            src_ref=send3.at[there],
+            dst_ref=recv3.at[partner],
+            send_sem=send_sems.at[3],
+            recv_sem=recv_sems.at[4 + dy],
+            device_id=(me, there),
+            device_id_type=MESH,
+        ).start()
+
     flat[...] = recv2[...].astype(F32).reshape(256, COLS)
     for half in range(2):
         gated = flat[pl.ds(half, COLS, stride=2), :].T * gate_in[half * 128 : half * 128 + 128]
         mean = jnp.mean(gated * gated, axis=1, keepdims=True)
         gated = gated * lax.rsqrt(mean + NORM_EPS) * gate_in[256:257]
         send3[4 * half : 4 * half + 4] = gated.reshape(4, 32, COLS).astype(BF)
+        if half == EAGER // 4:
+            pl.when(col != EAGER)(lambda: send_over(EAGER, lax.rem(EAGER // 2 + 4 - y, 4)))
 
     for (dy, _), there in zip(FAR_COLS, col_peers):
-        pltpu.make_async_remote_copy(
-            src_ref=send3.at[there],
-            dst_ref=recv3.at[partner],
-            send_sem=send_sems.at[4],
-            recv_sem=recv_sems.at[4 + dy],
-            device_id=(me, there),
-            device_id_type=MESH,
-        ).start()
+        pl.when(there != EAGER)(lambda there=there, dy=dy: send_over(there, dy))
     recv3[partner] = send3[col]
-    loads[21].wait()
-    for dy in (0, 1, 3, 2):
+    loaded((out_w, 14))
+    for dy in (0, 3, 2, 1):
         count = 2 if dy else 1
         pltpu.make_async_copy(
             recv3.at[pl.ds(0, count)], recv3.at[pl.ds(0, count)], recv_sems.at[4 + dy]
@@ -480,21 +475,18 @@
         part = dot(mixed, out_w[pl.ds(pl.multiple_of(source * 256, 256), 256), :])
         if dy == 0:
             total[...] = part
-        elif dy != 2:
+        elif dy != 1:
             total[...] += part
         else:
             out_ref[...] = (total[...] + part).astype(BF)
 
-    for number, source in ((2, send1.at[1]), (0, send1.at[0])):
-        pltpu.make_async_copy(
-            source.at[pl.ds(0, ROWS - 1)], source.at[pl.ds(0, ROWS - 1)], send_sems.at[number]
-        ).wait()
-    pltpu.make_async_copy(edge_out, edge_out, send_sems.at[1]).wait()
-    pltpu.make_async_copy(send2, send2, send_sems.at[3]).wait()
-    pltpu.make_async_copy(gate_own, gate_own, send_sems.at[5]).wait()
-    pltpu.make_async_copy(
-        send3.at[pl.ds(0, n_col - 1)], send3.at[pl.ds(0, n_col - 1)], send_sems.at[4]
-    ).wait()
+    for number, source in enumerate(
+        [
+            send1.at[:, pl.ds(0, ROWS - 1)], edge_out, send2, send3.at[pl.ds(0, n_col - 1)],
+            gate_own,
+        ]
+    ):
+        pltpu.make_async_copy(source, source, send_sems.at[number]).wait()
 
 
 def local(
@@ -509,14 +501,14 @@
         jnp.swapaxes(filter_weight, 2, 3), filter_skip, output_gain[None], output_weight,
     ] + [
         jnp.asarray(constants[name])
-        for name in ("first", "twiddle", "second", "back", "last", "feats")
+        for name in ("twiddle", "tables", "feats")
     ]
     vmem = pltpu.VMEM
-    scratch = (
-        [vmem(x.shape, x.dtype) for x in operands[0:2]]
-        + [vmem((WIDTH, 384), BF)]
-        + [vmem(x.shape, x.dtype) for x in operands[5:]]
-    )
+    scratch = [vmem(x.shape, x.dtype) for x in operands[0:2]]
+    scratch += [vmem((WIDTH, 384), BF)]
+    scratch += [vmem(x.shape, x.dtype) for x in operands[5:8]]
+    scratch += [vmem((3, 1, 64), F32), vmem((64, 64), F32)]
+    scratch += [vmem(x.shape, x.dtype) for x in operands[12:]]
     scratch += [
         vmem((256, WIDTH), BF),
         vmem((256, COLS), F32),
@@ -536,8 +528,8 @@
         vmem((2, 8, COLS), BF),
         vmem((2, 8, COLS), BF),
         vmem((32, WIDTH), F32),
-        pltpu.SemaphoreType.DMA((22,)),
-        pltpu.SemaphoreType.DMA((6,)),
+        pltpu.SemaphoreType.DMA((15,)),
+        pltpu.SemaphoreType.DMA((5,)),
         pltpu.SemaphoreType.DMA((9,)),
     ]
     return pl.pallas_call(

time: 29.8 us -> 29.2 us (0.980)
  Pallas kernels: 29.1 us -> 28.5 us
    pallas_call x1, Pallas kernels: 29.1 us -> 28.5 us  [local(): pl.pallas_call(kernel, out_shape=pltpu.VMEM((32, WIDTH), BF), in_specs=[p...]
where the time goes in v6:
time: 29.2 us
  Pallas kernels  28.5 us (98%)
  local copies, waits for them, and re-layouts  0.66 us (2%)
    pallas_call x1, Pallas kernels, local(): pl.pallas_call(kernel, out_shape=pltpu.VMEM((32, WIDTH), BF), in_specs=[p...  28.5 us
    unnamed x1, local copies, waits for them, and re-layouts  0.66 us

profile of v6, /device:TPU:1, one launch (start us, length us, event | category | flops | bytes accessed | tf_op | source)
XLA Modules:
  0.0 29.2 jit_solution(16356751816327185306)
XLA Ops:
  0.0 28.5 %shard_map.181 = bf16[32,2048]{1,0:T(8,128)(2,1)S(1)} custom-call(bf16[256,2048]{1,0:T(8,128)(2,1)} %tokens_hbm.1, f32[1,2048]{1,0:T(1,128)} %bitcast.6, bf16[2048,128]{1,0:T(8,128)(2,1)} %gate0_hbm.1, bf16[2048,128]{1,0:T(8,128)(2,1)} %gate1_hbm.1, bf16[2048,128]{1,0:T(8,128)(2,1)} %gate2_hbm.1, bf16[3,3,128]{2,1,0:T(4,128)(2,1)} %short_w_hbm.1, ...), custom_call_target="tpu_custom_call" | custom-call | tf_op jit(solution)/shard_map/pallas_call | solution.py:535
  28.5 0.7 %copy.21 = bf16[32,2048]{1,0:T(8,128)(2,1)} copy(bf16[32,2048]{1,0:T(8,128)(2,1)S(1)} %shard_map.181) | data formatting | bytes 262144

commit v7 on v6

--- a/solution.py
+++ b/solution.py
@@ -31,15 +31,17 @@
 
 
 def farthest_first(steps):
-    return [offset for _, offset in sorted(steps, reverse=True) if any(offset)]
-
-
-FAR_ROWS = farthest_first(
+    return [step for step in sorted(steps, reverse=True) if any(step[1])]
+
+
+ROW_HOPS = farthest_first(
     [(min(dz, 8 - dz) + min(dx, 4 - dx), (dz, dx)) for dz in range(8) for dx in range(4)]
 )
-FAR_COLS = farthest_first(
+FAR_ROWS = [offset for _, offset in ROW_HOPS]
+COL_HOPS = farthest_first(
     [(2 * min(dy, 4 - dy) + dc, (dy, dc)) for dy in range(4) for dc in range(2)]
 )
+FAR_COLS = [offset for _, offset in COL_HOPS]
 
 BF = jnp.bfloat16
 F32 = jnp.float32
@@ -167,6 +169,19 @@
     col = lax.axis_index("col")
     n_col = 8
 
+    def loaded(*targets):
+        for target, number in targets:
+            pltpu.make_async_copy(target, target, load_sem.at[number]).wait()
+
+    barrier = pltpu.get_barrier_semaphore()
+
+    z, x = lax.div(me, 4), lax.rem(me, 4)
+    row_peers = [lax.rem(z + dz, 8) * 4 + lax.rem(x + dx, 4) for dz, dx in FAR_ROWS]
+    y, core = lax.div(col, 2), lax.rem(col, 2)
+    partner = y * 2 + 1 - core
+    col_peers = [lax.rem(y + dy, 4) * 2 + lax.rem(core + dc, 2) for dy, dc in FAR_COLS]
+    for there in row_peers:
+        pl.semaphore_signal(barrier, inc=1, device_id=(there, col), device_id_type=MESH)
     copies = [
         (tokens_hbm, tokens, 0),
         (norm_gain_hbm, norm_gain, 1),
@@ -191,19 +206,6 @@
     for source, target, number in copies:
         pltpu.make_async_copy(source, target, load_sem.at[number]).start()
 
-    def loaded(*targets):
-        for target, number in targets:
-            pltpu.make_async_copy(target, target, load_sem.at[number]).wait()
-
-    barrier = pltpu.get_barrier_semaphore()
-
-    z, x = lax.div(me, 4), lax.rem(me, 4)
-    row_peers = [lax.rem(z + dz, 8) * 4 + lax.rem(x + dx, 4) for dz, dx in FAR_ROWS]
-    y, core = lax.div(col, 2), lax.rem(col, 2)
-    partner = y * 2 + 1 - core
-    col_peers = [lax.rem(y + dy, 4) * 2 + lax.rem(core + dc, 2) for dy, dc in FAR_COLS]
-    for there in row_peers:
-        pl.semaphore_signal(barrier, inc=1, device_id=(there, col), device_id_type=MESH)
     for there in col_peers:
         pl.semaphore_signal(barrier, inc=1, device_id=(me, there), device_id_type=MESH)
 
@@ -236,20 +238,19 @@
 
     pl.semaphore_wait(barrier, ROWS - 1 + n_col - 1)
 
-    def send_rows(source, target, number):
-        for there in row_peers:
-            pltpu.make_async_remote_copy(
-                src_ref=source.at[there],
-                dst_ref=target.at[me],
-                send_sem=send_sems.at[0],
-                recv_sem=recv_sems.at[number],
-                device_id=(there, col),
-                device_id_type=MESH,
-            ).start()
-        target[me] = source[me]
-
-    send_rows(send1.at[1], recv1.at[1], 2)
-    send_rows(send1.at[0], recv1.at[0], 0)
+    urgency = [(hops - 1 + b, b, k) for k, (hops, _) in enumerate(ROW_HOPS) for b in range(2)]
+    for _, b, k in sorted(urgency, key=lambda item: (-item[0], -item[1], item[2])):
+        there = row_peers[k]
+        pltpu.make_async_remote_copy(
+            src_ref=send1.at[b, there],
+            dst_ref=recv1.at[b, me],
+            send_sem=send_sems.at[0],
+            recv_sem=recv_sems.at[2 * b],
+            device_id=(there, col),
+            device_id_type=MESH,
+        ).start()
+    for b in range(2):
+        recv1[b, me] = send1[b, me]
     for side, there in ((0, lax.rem(me + 1, ROWS)), (1, lax.rem(me + ROWS - 1, ROWS))):
         pltpu.make_async_remote_copy(
             src_ref=edge_out.at[side],
@@ -353,7 +354,7 @@
         src_ref=gate_own,
         dst_ref=gate_in,
         send_sem=send_sems.at[4],
-        recv_sem=recv_sems.at[8],
+        recv_sem=recv_sems.at[4],
         device_id=(me, partner),
         device_id_type=MESH,
     ).start()
@@ -440,14 +441,14 @@
             device_id_type=MESH,
         ).start()
     pltpu.make_async_copy(recv2, recv2, recv_sems.at[3]).wait()
-    pltpu.make_async_copy(gate_in, gate_in, recv_sems.at[8]).wait()
-
-    def send_over(there, dy):
+    pltpu.make_async_copy(gate_in, gate_in, recv_sems.at[4]).wait()
+
+    def send_over(there, back):
         pltpu.make_async_remote_copy(
             src_ref=send3.at[there],
             dst_ref=recv3.at[partner],
             send_sem=send_sems.at[3],
-            recv_sem=recv_sems.at[4 + dy],
+            recv_sem=recv_sems.at[5 + back + core * (back // 3)],
             device_id=(me, there),
             device_id_type=MESH,
         ).start()
@@ -459,23 +460,31 @@
         gated = gated * lax.rsqrt(mean + NORM_EPS) * gate_in[256:257]
         send3[4 * half : 4 * half + 4] = gated.reshape(4, 32, COLS).astype(BF)
         if half == EAGER // 4:
-            pl.when(col != EAGER)(lambda: send_over(EAGER, lax.rem(EAGER // 2 + 4 - y, 4)))
+            pl.when(col != EAGER)(lambda: send_over(EAGER, lax.rem(y + 4 - EAGER // 2, 4)))
 
     for (dy, _), there in zip(FAR_COLS, col_peers):
-        pl.when(there != EAGER)(lambda there=there, dy=dy: send_over(there, dy))
+        pl.when(there != EAGER)(lambda there=there, dy=dy: send_over(there, (4 - dy) % 4))
     recv3[partner] = send3[col]
     loaded((out_w, 14))
-    for dy in (0, 3, 2, 1):
-        count = 2 if dy else 1
-        pltpu.make_async_copy(
-            recv3.at[pl.ds(0, count)], recv3.at[pl.ds(0, count)], recv_sems.at[4 + dy]
-        ).wait()
-        source = lax.rem(y + 4 - dy, 4)
+
+    def arrived(count, number):
+        block = recv3.at[pl.ds(0, count)]
+        pltpu.make_async_copy(block, block, recv_sems.at[number]).wait()
+
+    for back in range(3):
+        arrived(2 if back else 1, 5 + back)
+        source = lax.rem(y + back, 4)
         mixed = jnp.concatenate([recv3[2 * source], recv3[2 * source + 1]], axis=1)
         part = dot(mixed, out_w[pl.ds(pl.multiple_of(source * 256, 256), 256), :])
-        if dy == 0:
+        if back == 0:
             total[...] = part
-        elif dy != 1:
+        else:
+            total[...] += part
+    for sender in range(2):
+        arrived(1, 8 + sender)
+        group = 2 * lax.rem(y + 3, 4) + 1 - sender
+        part = dot(recv3[group], out_w[pl.ds(pl.multiple_of(group * 128, 128), 128), :])
+        if sender == 0:
             total[...] += part
         else:
             out_ref[...] = (total[...] + part).astype(BF)
@@ -530,7 +539,7 @@
         vmem((32, WIDTH), F32),
         pltpu.SemaphoreType.DMA((15,)),
         pltpu.SemaphoreType.DMA((5,)),
-        pltpu.SemaphoreType.DMA((9,)),
+        pltpu.SemaphoreType.DMA((10,)),
     ]
     return pl.pallas_call(
         kernel,

time: 29.2 us -> 29.1 us (level)
  no operation moved by 1% of the time
where the time goes in v7:
time: 29.1 us; the launch traced here: 29 us
  Pallas kernels  28.4 us (98%)
  local copies, waits for them, and re-layouts  0.66 us (2%)
    pallas_call x1, Pallas kernels, local(): pl.pallas_call(kernel, out_shape=pltpu.VMEM((32, WIDTH), BF), in_specs=[p...  28.4 us
    unnamed x1, local copies, waits for them, and re-layouts  0.66 us

profile of v7, /device:TPU:1, one launch (start us, length us, event | category | flops | bytes accessed | tf_op | source)
XLA Modules:
  0.0 29.0 jit_solution(17836006679765566694)
XLA Ops:
  0.0 28.4 %shard_map.181 = bf16[32,2048]{1,0:T(8,128)(2,1)S(1)} custom-call(bf16[256,2048]{1,0:T(8,128)(2,1)} %tokens_hbm.1, f32[1,2048]{1,0:T(1,128)} %bitcast.6, bf16[2048,128]{1,0:T(8,128)(2,1)} %gate0_hbm.1, bf16[2048,128]{1,0:T(8,128)(2,1)} %gate1_hbm.1, bf16[2048,128]{1,0:T(8,128)(2,1)} %gate2_hbm.1, bf16[3,3,128]{2,1,0:T(4,128)(2,1)} %short_w_hbm.1, ...), custom_call_target="tpu_custom_call" | custom-call | tf_op jit(solution)/shard_map/pallas_call | solution.py:544
  28.4 0.7 %copy.21 = bf16[32,2048]{1,0:T(8,128)(2,1)} copy(bf16[32,2048]{1,0:T(8,128)(2,1)S(1)} %shard_map.181) | data formatting | bytes 262144

commit v8 on v7

--- a/solution.py
+++ b/solution.py
@@ -160,10 +160,10 @@
     embed_w_hbm, embed_b_hbm, inner_w_hbm, inner_b_hbm, freq_hbm, filter_w_hbm, skip_hbm,
     out_gain_hbm, out_w_hbm, twiddle_hbm, tables_hbm, feats_hbm,
     out_ref,
-    tokens, norm_gain, gates, short_w, short_b, embed_w, lines, inner_w,
-    filter_w, skip, out_gain, out_w, twiddle, tables, feats,
+    tokens, gains, gates, short_w, short_b, layers, lines,
+    filter_w, skip, out_w, twiddle, tables, feats,
     normed, flat, packed, send1, recv1, params, mixed_taps, spectra, smooth,
-    send2, recv2, send3, recv3, gate_own, gate_in, edge_out, edge_in, total, load_sem, send_sems, recv_sems,
+    send2, recv2, send3, recv3, gate_own, gate_in, gate_rows, edge_out, edge_in, total, load_sem, send_sem, recv_sems,
 ):
     me = lax.axis_index("row")
     col = lax.axis_index("col")
@@ -184,15 +184,15 @@
         pl.semaphore_signal(barrier, inc=1, device_id=(there, col), device_id_type=MESH)
     copies = [
         (tokens_hbm, tokens, 0),
-        (norm_gain_hbm, norm_gain, 1),
+        (norm_gain_hbm, gains.at[:, 0:WIDTH], 1),
         (gate0_hbm, gates.at[:, 0:128], 2),
         (gate1_hbm, gates.at[:, 128:256], 2),
         (gate2_hbm, gates.at[:, 256:384], 2),
-        (embed_w_hbm, embed_w, 3),
+        (embed_w_hbm, layers.at[64:97], 3),
         (embed_b_hbm, lines.at[0], 4),
         (inner_b_hbm, lines.at[1], 4),
         (freq_hbm, lines.at[2], 4),
-        (inner_w_hbm, inner_w, 5),
+        (inner_w_hbm, layers.at[0:64], 3),
         (filter_w_hbm, filter_w, 6),
         (feats_hbm, feats, 7),
         (tables_hbm, tables, 8),
@@ -200,8 +200,8 @@
         (short_w_hbm, short_w, 10),
         (short_b_hbm, short_b, 11),
         (skip_hbm, skip, 12),
-        (out_gain_hbm, out_gain, 13),
-        (out_w_hbm, out_w, 14),
+        (out_gain_hbm, gains.at[:, WIDTH : WIDTH + COLS], 1),
+        (out_w_hbm, out_w, 5),
     ]
     for source, target, number in copies:
         pltpu.make_async_copy(source, target, load_sem.at[number]).start()
@@ -209,13 +209,13 @@
     for there in col_peers:
         pl.semaphore_signal(barrier, inc=1, device_id=(me, there), device_id_type=MESH)
 
-    loaded((tokens, 0), (norm_gain, 1))
+    loaded((tokens, 0), (gains, 1))
 
     def normalise(j, carry):
         rows = pl.ds(pl.multiple_of(j * 64, 64), 64)
         wide_tokens = tokens[rows, :].astype(F32)
         mean = jnp.mean(wide_tokens * wide_tokens, axis=1, keepdims=True)
-        normed[rows, :] = (wide_tokens * lax.rsqrt(mean + NORM_EPS) * norm_gain[...]).astype(BF)
+        normed[rows, :] = (wide_tokens * lax.rsqrt(mean + NORM_EPS) * gains[:, 0:WIDTH]).astype(BF)
         return carry
 
     lax.fori_loop(0, 4, normalise, 0)
@@ -244,7 +244,7 @@
         pltpu.make_async_remote_copy(
             src_ref=send1.at[b, there],
             dst_ref=recv1.at[b, me],
-            send_sem=send_sems.at[0],
+            send_sem=send_sem,
             recv_sem=recv_sems.at[2 * b],
             device_id=(there, col),
             device_id_type=MESH,
@@ -255,20 +255,20 @@
         pltpu.make_async_remote_copy(
             src_ref=edge_out.at[side],
             dst_ref=edge_in.at[side],
-            send_sem=send_sems.at[1],
+            send_sem=send_sem,
             recv_sem=recv_sems.at[1],
             device_id=(there, col),
             device_id_type=MESH,
         ).start()
 
-    loaded((embed_w, 3), (lines, 4), (inner_w, 5), (filter_w, 6), (feats, 7), (tables, 8))
+    loaded((layers, 3), (lines, 4), (filter_w, 6), (feats, 7), (tables, 8))
     loaded((twiddle, 9))
     params[...] = jnp.zeros_like(params)
     scale = lines[2] * (1.0 / (2.0 * math.pi))
-    params[0:33, 0:64] = embed_w[...] * scale
+    params[0:33, 0:64] = layers[64:97] * scale
     params[33:34, 0:64] = lines[0] * scale - 0.25
     params[48:49, 0:64] = lines[1] * scale - 0.25
-    params[64:128, 0:64] = inner_w[...] * scale
+    params[64:128, 0:64] = layers[0:64] * scale
     turned = params[...].T
     embed_t = wide(turned[0:64, 0:FEATS])
     inner_bias = turned[0:64, 48:49]
@@ -319,7 +319,7 @@
                 tables[0:256, part * COLS : (part + 1) * COLS],
             )
 
-    loaded((short_w, 10), (short_b, 11), (skip, 12), (out_gain, 13))
+    loaded((short_w, 10), (short_b, 11), (skip, 12))
     lane8 = lax.broadcasted_iota(jnp.int32, (8, COLS), 1)
     mine = lane8 == OWN * me + lax.rem(lax.broadcasted_iota(jnp.int32, (8, COLS), 0), OWN)
 
@@ -349,11 +349,11 @@
     value = short_b[1:2, :] + before * all_short[1, 0:1]
     value = value + here * all_short[1, 1:2]
     gate_own[0:256, :] = value + after * all_short[1, 2:3]
-    gate_own[256:264, :] = jnp.broadcast_to(out_gain[...], (8, COLS))
+    gate_own[256:264, :] = jnp.broadcast_to(gains[:, WIDTH : WIDTH + COLS], (8, COLS))
     pltpu.make_async_remote_copy(
         src_ref=gate_own,
         dst_ref=gate_in,
-        send_sem=send_sems.at[4],
+        send_sem=send_sem,
         recv_sem=recv_sems.at[4],
         device_id=(me, partner),
         device_id_type=MESH,
@@ -435,29 +435,38 @@
         pltpu.make_async_remote_copy(
             src_ref=send2.at[there],
             dst_ref=recv2.at[me],
-            send_sem=send_sems.at[2],
+            send_sem=send_sem,
             recv_sem=recv_sems.at[3],
             device_id=(there, partner),
             device_id_type=MESH,
         ).start()
+    pltpu.make_async_copy(gate_in, gate_in, recv_sems.at[4]).wait()
+    gain = jnp.broadcast_to(gate_in[256:257], (COLS, COLS)).T
+    for half in range(2):
+        gate_rows[0, pl.ds(half, COLS, stride=2), :] = gate_in[half * 128 : half * 128 + 128].T
+        gate_rows[1, pl.ds(half, COLS, stride=2), :] = gain
+
     pltpu.make_async_copy(recv2, recv2, recv_sems.at[3]).wait()
-    pltpu.make_async_copy(gate_in, gate_in, recv_sems.at[4]).wait()
 
     def send_over(there, back):
         pltpu.make_async_remote_copy(
             src_ref=send3.at[there],
             dst_ref=recv3.at[partner],
-            send_sem=send_sems.at[3],
+            send_sem=send_sem,
             recv_sem=recv_sems.at[5 + back + core * (back // 3)],
             device_id=(me, there),
             device_id_type=MESH,
         ).start()
 
-    flat[...] = recv2[...].astype(F32).reshape(256, COLS)
+    gated = recv2[...].astype(F32) * gate_rows[0].reshape(ROWS, 8, COLS)
+    squares = jnp.sum(gated * gated, axis=0)
+    squares = squares + pltpu.roll(squares, 4, axis=0)
+    squares = squares + pltpu.roll(squares, 2, axis=0)
+    factor = lax.rsqrt(squares * (GROUPS / CHANNELS) + NORM_EPS)
+    gated = gated * factor[None] * gate_rows[1].reshape(ROWS, 8, COLS)
+    flat[...] = gated.reshape(256, COLS)
     for half in range(2):
-        gated = flat[pl.ds(half, COLS, stride=2), :].T * gate_in[half * 128 : half * 128 + 128]
-        mean = jnp.mean(gated * gated, axis=1, keepdims=True)
-        gated = gated * lax.rsqrt(mean + NORM_EPS) * gate_in[256:257]
+        gated = flat[pl.ds(half, COLS, stride=2), :].T
         send3[4 * half : 4 * half + 4] = gated.reshape(4, 32, COLS).astype(BF)
         if half == EAGER // 4:
             pl.when(col != EAGER)(lambda: send_over(EAGER, lax.rem(y + 4 - EAGER // 2, 4)))
@@ -465,7 +474,7 @@
     for (dy, _), there in zip(FAR_COLS, col_peers):
         pl.when(there != EAGER)(lambda there=there, dy=dy: send_over(there, (4 - dy) % 4))
     recv3[partner] = send3[col]
-    loaded((out_w, 14))
+    loaded((out_w, 5))
 
     def arrived(count, number):
         block = recv3.at[pl.ds(0, count)]
@@ -489,13 +498,8 @@
         else:
             out_ref[...] = (total[...] + part).astype(BF)
 
-    for number, source in enumerate(
-        [
-            send1.at[:, pl.ds(0, ROWS - 1)], edge_out, send2, send3.at[pl.ds(0, n_col - 1)],
-            gate_own,
-        ]
-    ):
-        pltpu.make_async_copy(source, source, send_sems.at[number]).wait()
+    sent = mixed_taps.at[pl.ds(0, 760)]
+    pltpu.make_async_copy(sent, sent, send_sem).wait()
 
 
 def local(
@@ -513,11 +517,10 @@
         for name in ("twiddle", "tables", "feats")
     ]
     vmem = pltpu.VMEM
-    scratch = [vmem(x.shape, x.dtype) for x in operands[0:2]]
-    scratch += [vmem((WIDTH, 384), BF)]
-    scratch += [vmem(x.shape, x.dtype) for x in operands[5:8]]
-    scratch += [vmem((3, 1, 64), F32), vmem((64, 64), F32)]
-    scratch += [vmem(x.shape, x.dtype) for x in operands[12:]]
+    scratch = [vmem(tokens.shape, BF), vmem((1, WIDTH + COLS), F32), vmem((WIDTH, 384), BF)]
+    scratch += [vmem(x.shape, x.dtype) for x in operands[5:7]]
+    scratch += [vmem((97, 64), F32), vmem((3, 1, 64), F32)]
+    scratch += [vmem(x.shape, x.dtype) for x in operands[12:14] + operands[15:]]
     scratch += [
         vmem((256, WIDTH), BF),
         vmem((256, COLS), F32),
@@ -534,11 +537,12 @@
         vmem((8, 32, COLS), BF),
         vmem((264, COLS), F32),
         vmem((264, COLS), F32),
+        vmem((2, 256, COLS), F32),
         vmem((2, 8, COLS), BF),
         vmem((2, 8, COLS), BF),
         vmem((32, WIDTH), F32),
-        pltpu.SemaphoreType.DMA((15,)),
-        pltpu.SemaphoreType.DMA((5,)),
+        pltpu.SemaphoreType.DMA((13,)),
+        pltpu.SemaphoreType.DMA(()),
         pltpu.SemaphoreType.DMA((10,)),
     ]
     return pl.pallas_call(

time: 29.1 us -> 29 us (level)
  no operation moved by 1% of the time
where the time goes in v8:
time: 29 us
  Pallas kernels  28.3 us (98%)
  local copies, waits for them, and re-layouts  0.66 us (2%)
    pallas_call x1, Pallas kernels, local(): pl.pallas_call(kernel, out_shape=pltpu.VMEM((32, WIDTH), BF), in_specs=[p...  28.3 us
    unnamed x1, local copies, waits for them, and re-layouts  0.66 us

profile of v8, /device:TPU:1, one launch (start us, length us, event | category | flops | bytes accessed | tf_op | source)
XLA Modules:
  0.0 29.0 jit_solution(13599916351452300572)
XLA Ops:
  0.0 28.3 %shard_map.181 = bf16[32,2048]{1,0:T(8,128)(2,1)S(1)} custom-call(bf16[256,2048]{1,0:T(8,128)(2,1)} %tokens_hbm.1, f32[1,2048]{1,0:T(1,128)} %bitcast.6, bf16[2048,128]{1,0:T(8,128)(2,1)} %gate0_hbm.1, bf16[2048,128]{1,0:T(8,128)(2,1)} %gate1_hbm.1, bf16[2048,128]{1,0:T(8,128)(2,1)} %gate2_hbm.1, bf16[3,3,128]{2,1,0:T(4,128)(2,1)} %short_w_hbm.1, ...), custom_call_target="tpu_custom_call" | custom-call | tf_op jit(solution)/shard_map/pallas_call | solution.py:548
  28.3 0.7 %copy.21 = bf16[32,2048]{1,0:T(8,128)(2,1)} copy(bf16[32,2048]{1,0:T(8,128)(2,1)S(1)} %shard_map.181) | data formatting | bytes 262144

commit v9 on v8

--- a/solution.py
+++ b/solution.py
@@ -338,26 +338,6 @@
         pltpu.make_async_copy(
             target.at[pl.ds(0, ROWS - 1)], target.at[pl.ds(0, ROWS - 1)], recv_sems.at[number]
         ).wait()
-
-    pltpu.make_async_copy(edge_in, edge_in, recv_sems.at[1]).wait()
-    position = lax.broadcasted_iota(jnp.int32, (256, COLS), 0)
-    here = gate_own[0:256, :]
-    first_edge = edge_in[0].astype(F32)[7:8] * jnp.where(me == 0, 0.0, 1.0)
-    last_edge = edge_in[1].astype(F32)[0:1] * jnp.where(me == ROWS - 1, 0.0, 1.0)
-    before = jnp.where(position == 0, first_edge, pltpu.roll(here, 1, axis=0))
-    after = jnp.where(position == 255, last_edge, pltpu.roll(here, 255, axis=0))
-    value = short_b[1:2, :] + before * all_short[1, 0:1]
-    value = value + here * all_short[1, 1:2]
-    gate_own[0:256, :] = value + after * all_short[1, 2:3]
-    gate_own[256:264, :] = jnp.broadcast_to(gains[:, WIDTH : WIDTH + COLS], (8, COLS))
-    pltpu.make_async_remote_copy(
-        src_ref=gate_own,
-        dst_ref=gate_in,
-        send_sem=send_sem,
-        recv_sem=recv_sems.at[4],
-        device_id=(me, partner),
-        device_id_type=MESH,
-    ).start()
 
     row = lax.broadcasted_iota(jnp.int32, (256, COLS), 0)
     lane = lax.broadcasted_iota(jnp.int32, (256, COLS), 1)
@@ -440,6 +420,26 @@
             device_id=(there, partner),
             device_id_type=MESH,
         ).start()
+    pltpu.make_async_copy(edge_in, edge_in, recv_sems.at[1]).wait()
+    position = lax.broadcasted_iota(jnp.int32, (256, COLS), 0)
+    here = gate_own[0:256, :]
+    first_edge = edge_in[0].astype(F32)[7:8] * jnp.where(me == 0, 0.0, 1.0)
+    last_edge = edge_in[1].astype(F32)[0:1] * jnp.where(me == ROWS - 1, 0.0, 1.0)
+    before = jnp.where(position == 0, first_edge, pltpu.roll(here, 1, axis=0))
+    after = jnp.where(position == 255, last_edge, pltpu.roll(here, 255, axis=0))
+    value = short_b[1:2, :] + before * all_short[1, 0:1]
+    value = value + here * all_short[1, 1:2]
+    gate_own[0:256, :] = value + after * all_short[1, 2:3]
+    gate_own[256:264, :] = jnp.broadcast_to(gains[:, WIDTH : WIDTH + COLS], (8, COLS))
+    pltpu.make_async_remote_copy(
+        src_ref=gate_own,
+        dst_ref=gate_in,
+        send_sem=send_sem,
+        recv_sem=recv_sems.at[4],
+        device_id=(me, partner),
+        device_id_type=MESH,
+    ).start()
+
     pltpu.make_async_copy(gate_in, gate_in, recv_sems.at[4]).wait()
     gain = jnp.broadcast_to(gate_in[256:257], (COLS, COLS)).T
     for half in range(2):

time: 29 us -> 29 us (level)
  no operation moved by 1% of the time
where the time goes in v9:
time: 29 us
  Pallas kernels  28.3 us (98%)
  local copies, waits for them, and re-layouts  0.66 us (2%)
    pallas_call x1, Pallas kernels, local(): pl.pallas_call(kernel, out_shape=pltpu.VMEM((32, WIDTH), BF), in_specs=[p...  28.3 us
    unnamed x1, local copies, waits for them, and re-layouts  0.66 us

profile of v9, /device:TPU:1, one launch (start us, length us, event | category | flops | bytes accessed | tf_op | source)
XLA Modules:
  0.0 29.0 jit_solution(2007912274480462871)
XLA Ops:
  0.0 28.3 %shard_map.181 = bf16[32,2048]{1,0:T(8,128)(2,1)S(1)} custom-call(bf16[256,2048]{1,0:T(8,128)(2,1)} %tokens_hbm.1, f32[1,2048]{1,0:T(1,128)} %bitcast.6, bf16[2048,128]{1,0:T(8,128)(2,1)} %gate0_hbm.1, bf16[2048,128]{1,0:T(8,128)(2,1)} %gate1_hbm.1, bf16[2048,128]{1,0:T(8,128)(2,1)} %gate2_hbm.1, bf16[3,3,128]{2,1,0:T(4,128)(2,1)} %short_w_hbm.1, ...), custom_call_target="tpu_custom_call" | custom-call | tf_op jit(solution)/shard_map/pallas_call | solution.py:548
  28.3 0.7 %copy.21 = bf16[32,2048]{1,0:T(8,128)(2,1)} copy(bf16[32,2048]{1,0:T(8,128)(2,1)S(1)} %shard_map.181) | data formatting | bytes 262144

commit v10 on v9

--- a/solution.py
+++ b/solution.py
@@ -480,20 +480,21 @@
         block = recv3.at[pl.ds(0, count)]
         pltpu.make_async_copy(block, block, recv_sems.at[number]).wait()
 
-    for back in range(3):
-        arrived(2 if back else 1, 5 + back)
+    for back, sender in ((0, None), (1, None), (3, 0), (2, None), (3, 1)):
         source = lax.rem(y + back, 4)
-        mixed = jnp.concatenate([recv3[2 * source], recv3[2 * source + 1]], axis=1)
-        part = dot(mixed, out_w[pl.ds(pl.multiple_of(source * 256, 256), 256), :])
+        if sender is None:
+            arrived(2 if back else 1, 5 + back)
+            mixed = jnp.concatenate([recv3[2 * source], recv3[2 * source + 1]], axis=1)
+            rows = pl.ds(pl.multiple_of(source * 256, 256), 256)
+        else:
+            arrived(1, 8 + sender)
+            group = 2 * source + 1 - sender
+            mixed = recv3[group]
+            rows = pl.ds(pl.multiple_of(group * 128, 128), 128)
+        part = dot(mixed, out_w[rows, :])
         if back == 0:
             total[...] = part
-        else:
-            total[...] += part
-    for sender in range(2):
-        arrived(1, 8 + sender)
-        group = 2 * lax.rem(y + 3, 4) + 1 - sender
-        part = dot(recv3[group], out_w[pl.ds(pl.multiple_of(group * 128, 128), 128), :])
-        if sender == 0:
+        elif sender != 1:
             total[...] += part
         else:
             out_ref[...] = (total[...] + part).astype(BF)

time: 29 us -> 29 us (level)
  no operation moved by 1% of the time
where the time goes in v10:
time: 29 us; the launch traced here: 28.9 us
  Pallas kernels  28.2 us (97%)
  local copies, waits for them, and re-layouts  0.66 us (2%)
    pallas_call x1, Pallas kernels, local(): pl.pallas_call(kernel, out_shape=pltpu.VMEM((32, WIDTH), BF), in_specs=[p...  28.2 us
    unnamed x1, local copies, waits for them, and re-layouts  0.66 us

profile of v10, /device:TPU:1, one launch (start us, length us, event | category | flops | bytes accessed | tf_op | source)
XLA Modules:
  0.0 28.9 jit_solution(667635878586147165)
XLA Ops:
  0.0 28.2 %shard_map.181 = bf16[32,2048]{1,0:T(8,128)(2,1)S(1)} custom-call(bf16[256,2048]{1,0:T(8,128)(2,1)} %tokens_hbm.1, f32[1,2048]{1,0:T(1,128)} %bitcast.6, bf16[2048,128]{1,0:T(8,128)(2,1)} %gate0_hbm.1, bf16[2048,128]{1,0:T(8,128)(2,1)} %gate1_hbm.1, bf16[2048,128]{1,0:T(8,128)(2,1)} %gate2_hbm.1, bf16[3,3,128]{2,1,0:T(4,128)(2,1)} %short_w_hbm.1, ...), custom_call_target="tpu_custom_call" | custom-call | tf_op jit(solution)/shard_map/pallas_call | solution.py:549
  28.2 0.7 %copy.21 = bf16[32,2048]{1,0:T(8,128)(2,1)} copy(bf16[32,2048]{1,0:T(8,128)(2,1)S(1)} %shard_map.181) | data formatting | bytes 262144

commit v11 on v10

--- a/solution.py
+++ b/solution.py
@@ -411,7 +411,7 @@
             ]
     send2[...] = packed[...].reshape(ROWS, 8, COLS).astype(BF)
 
-    for there in row_peers + [me]:
+    def send_back(there):
         pltpu.make_async_remote_copy(
             src_ref=send2.at[there],
             dst_ref=recv2.at[me],
@@ -420,6 +420,10 @@
             device_id=(there, partner),
             device_id_type=MESH,
         ).start()
+
+    send_back(0)
+    for there in row_peers + [me]:
+        pl.when(there != 0)(lambda there=there: send_back(there))
     pltpu.make_async_copy(edge_in, edge_in, recv_sems.at[1]).wait()
     position = lax.broadcasted_iota(jnp.int32, (256, COLS), 0)
     here = gate_own[0:256, :]

time: 29 us -> 29 us (level)
  no operation moved by 1% of the time
where the time goes in v11:
time: 29 us; the launch traced here: 28.9 us
  Pallas kernels  28.2 us (97%)
  local copies, waits for them, and re-layouts  0.66 us (2%)
    pallas_call x1, Pallas kernels, local(): pl.pallas_call(kernel, out_shape=pltpu.VMEM((32, WIDTH), BF), in_specs=[p...  28.2 us
    unnamed x1, local copies, waits for them, and re-layouts  0.66 us

profile of v11, /device:TPU:1, one launch (start us, length us, event | category | flops | bytes accessed | tf_op | source)
XLA Modules:
  0.0 28.9 jit_solution(4991321305943164456)
XLA Ops:
  0.0 28.2 %shard_map.181 = bf16[32,2048]{1,0:T(8,128)(2,1)S(1)} custom-call(bf16[256,2048]{1,0:T(8,128)(2,1)} %tokens_hbm.1, f32[1,2048]{1,0:T(1,128)} %bitcast.6, bf16[2048,128]{1,0:T(8,128)(2,1)} %gate0_hbm.1, bf16[2048,128]{1,0:T(8,128)(2,1)} %gate1_hbm.1, bf16[2048,128]{1,0:T(8,128)(2,1)} %gate2_hbm.1, bf16[3,3,128]{2,1,0:T(4,128)(2,1)} %short_w_hbm.1, ...), custom_call_target="tpu_custom_call" | custom-call | tf_op jit(solution)/shard_map/pallas_call | solution.py:553
  28.2 0.7 %copy.21 = bf16[32,2048]{1,0:T(8,128)(2,1)} copy(bf16[32,2048]{1,0:T(8,128)(2,1)S(1)} %shard_map.181) | data formatting | bytes 262144

commit v12 on v11

--- a/solution.py
+++ b/solution.py
@@ -361,7 +361,7 @@
             [smooth[b, pl.ds(i, LIVE, stride=OWN), :] for i in range(OWN)], axis=1
         )
 
-    pairs = 2
+    pairs = 4
     value = smoothed(1)
     signals = [value[:, p * COLS : (p + pairs) * COLS] for p in range(0, OWN, pairs)]
     for o in range(2):

time: 29 us -> 29 us (level)
  no operation moved by 1% of the time
where the time goes in v12:
time: 29 us; the launch traced here: 28.9 us
  Pallas kernels  28.2 us (97%)
  local copies, waits for them, and re-layouts  0.66 us (2%)
    pallas_call x1, Pallas kernels, local(): pl.pallas_call(kernel, out_shape=pltpu.VMEM((32, WIDTH), BF), in_specs=[p...  28.2 us
    unnamed x1, local copies, waits for them, and re-layouts  0.66 us

profile of v12, /device:TPU:1, one launch (start us, length us, event | category | flops | bytes accessed | tf_op | source)
XLA Modules:
  0.0 28.9 jit_solution(6161704670438061644)
XLA Ops:
  0.0 28.2 %shard_map.181 = bf16[32,2048]{1,0:T(8,128)(2,1)S(1)} custom-call(bf16[256,2048]{1,0:T(8,128)(2,1)} %tokens_hbm.1, f32[1,2048]{1,0:T(1,128)} %bitcast.6, bf16[2048,128]{1,0:T(8,128)(2,1)} %gate0_hbm.1, bf16[2048,128]{1,0:T(8,128)(2,1)} %gate1_hbm.1, bf16[2048,128]{1,0:T(8,128)(2,1)} %gate2_hbm.1, bf16[3,3,128]{2,1,0:T(4,128)(2,1)} %short_w_hbm.1, ...), custom_call_target="tpu_custom_call" | custom-call | tf_op jit(solution)/shard_map/pallas_call | solution.py:553
  28.2 0.7 %copy.21 = bf16[32,2048]{1,0:T(8,128)(2,1)} copy(bf16[32,2048]{1,0:T(8,128)(2,1)S(1)} %shard_map.181) | data formatting | bytes 262144
